TPU v7x, 32 devices: a whole 2x2x4 slice. The times are simulated.
32 devices in a mesh: sp: 16 (over z, y, x), tp: 2 (over core).
Axes of the slice: x: 2, y: 2, z: 4, core: 2. Of those that a mesh axis runs over, the one named last changes fastest.
Arguments:
- skip_stream_entering: bfloat16 [2048, 2048], P(('sp', 'tp')), may hold values from -6 to 6
- content_signal_matrix: bfloat16 [2048, 4096], P('sp', 'tp'), may hold values from -6 to 6
- writer_signal_matrix: bfloat16 [2048, 1024], P('sp', 'tp'), may hold values from -6 to 6
- reader_signal_matrix: bfloat16 [2048, 1024], P('sp', 'tp'), may hold values from -6 to 6
- multiplier_signal: bfloat16 [2048, 4096], P('sp', 'tp'), may hold values from -6 to 6
- interval_before_softplus: float32 [64, 2048], P('tp', 'sp'), may hold values from -7.5 to 0.5
- extra_log_shrink: float32 [64, 2048], P('tp', 'sp'), may hold values from -2.8 to 0
- log_forget_speed: float32 [64], P('tp'), may hold values from -12 to 0
- content_filter_coefs: bfloat16 [4, 4096], P(None, 'tp'), may hold values from -3 to 3
- writer_filter_coefs: bfloat16 [4, 1024], P(None, 'tp'), may hold values from -3 to 3
- reader_filter_coefs: bfloat16 [4, 1024], P(None, 'tp'), may hold values from -3 to 3
- skip_path_factor: float32 [64], P('tp'), may hold values from 0.25 to 2
- cluster_scaling_vector: float32 [4096], P('tp'), may hold values from 0.1 to 1.9
- blend_result_matrix: bfloat16 [4096, 2048], P('tp'), may hold values from -0.09375 to 0.09375
- feature_blend_scaling: float32 [2048], replicated, may hold values from 0.1 to 1.9
- widening_matrix: bfloat16 [2048, 8192], P('sp', 'tp'), may hold values from -0.125 to 0.125
- narrowing_matrix: bfloat16 [8192, 2048], P('tp', 'sp'), may hold values from -0.0625 to 0.0625
Outputs:
- layer_out: bfloat16 [2048, 2048], P(('sp', 'tp'))
All inputs are finite; a program needn't handle non-finite values.
Results may differ from a plain program's by a relative error of at most 0.02.
Values may be sent and summed in bfloat16 or wider, within the bound.
A program may use at most 128 MiB of HBM per device.

v0:
```python
import math
import jax
import jax.numpy as jnp
from jax import lax
from jax.experimental import pallas as pl
from jax.sharding import PartitionSpec as P

HEAD_DIM = 64
STATE = 128
BLOCK = 128


epsilon = 1e-05
precise = lax.Precision.HIGHEST
SP = ("sa", "sb")
TEAM = 8


def shifted(value, axis, steps):
    count = lax.axis_size(axis)
    initial, last = (max(0, -steps), min(count, count - steps))
    return lax.ppermute(value, axis, [(source, source + steps) for source in range(initial, last)])


def scan_rows(parts, factors, entering):
    def one(place, carried):
        entering[place] = carried.astype(jnp.bfloat16)
        return carried * factors[place] + parts[place].astype(jnp.float32)

    lax.fori_loop(0, parts.shape[0], one, jnp.zeros(parts.shape[1:], jnp.float32))


def prefix(log_total, end_state, rider):
    shards = lax.axis_size(SP)
    heads = end_state.shape[0] * end_state.shape[1]
    state_width = end_state.shape[-1]
    rows = end_state.reshape(-1, state_width).astype(jnp.bfloat16)
    count = rows.shape[0] // shards
    decays = jnp.repeat(jnp.exp(log_total).reshape(heads), rows.shape[0] // heads)
    extra = -(-count // state_width) * 16
    decays = decays.astype(jnp.bfloat16).reshape(shards, count)
    decays = jnp.pad(decays, ((0, 0), (0, extra * state_width - count)))
    packed = jnp.concatenate(
        [rows.reshape(shards, count, state_width), decays.reshape(shards, extra, state_width)],
        axis=1,
    )
    packed = lax.all_to_all(packed, SP, split_axis=0, concat_axis=0)
    parts = packed[:, :count]
    factors = packed[:, count:].reshape(shards, -1)[:, :count].astype(jnp.float32)
    entering = pl.pallas_call(
        scan_rows,
        out_shape=jax.ShapeDtypeStruct(parts.shape, jnp.bfloat16),
    )(parts, jnp.broadcast_to(factors[..., None], parts.shape))
    entering, rider = lax.optimization_barrier((entering, rider))
    back = lax.all_to_all(
        entering.reshape(rows.shape), SP, split_axis=0, concat_axis=0, tiled=True
    )
    return back.reshape(end_state.shape).astype(jnp.float32), rider


def summed_share(partial, axis):
    count = lax.axis_size(axis)
    if count != 2:
        return lax.psum_scatter(partial, axis, scatter_dimension=0, tiled=True)
    me = lax.axis_index(axis)
    length = partial.shape[0] // 2
    away = lax.dynamic_slice_in_dim(partial, (1 - me) * length, length, 0)
    kept = lax.dynamic_slice_in_dim(partial, me * length, length, 0)
    arrived = lax.ppermute(away, axis, [(0, 1), (1, 0)])
    return (kept.astype(jnp.float32) + arrived.astype(jnp.float32)).astype(jnp.bfloat16)


def convolve(inputs, rim_rows, conv_taps):
    width = conv_taps.shape[0]
    length = inputs.shape[0]
    extended = jnp.concatenate([rim_rows, inputs], axis=0)
    summed = extended[0:length].astype(jnp.float32) * conv_taps[0].astype(jnp.float32)
    for offset in range(1, width):
        summed = summed + extended[offset : offset + length].astype(jnp.float32) * conv_taps[
            offset
        ].astype(jnp.float32)
    return jax.nn.silu(summed)


def advance(carried, pair):
    block_state, block_factor = pair
    return (carried * block_factor[..., None, None] + block_state, carried)


def blockwise(values, interval_lengths, log_forgetting, key_rows, query_rows):
    length, groups, per_group, width = values.shape
    blocks = length // BLOCK
    value_blocks = values.reshape(blocks, BLOCK, groups, per_group, width)
    step_blocks = jnp.transpose(
        interval_lengths.reshape(groups, per_group, blocks, BLOCK), (2, 3, 0, 1)
    )
    weighted = value_blocks * step_blocks[..., None]
    cumulative = jnp.cumsum(
        jnp.transpose(log_forgetting.reshape(groups, per_group, blocks, BLOCK), (2, 0, 1, 3)),
        axis=-1,
    )
    key_blocks = key_rows.reshape(blocks, BLOCK, groups, -1)
    query_blocks = query_rows.reshape(blocks, BLOCK, groups, -1)
    causal = jnp.tril(jnp.ones((BLOCK, BLOCK), dtype=bool))
    decay_mask = jnp.exp(
        jnp.where(causal, cumulative[..., :, None] - cumulative[..., None, :], -jnp.inf)
    )
    scores = jnp.einsum("clgn,csgn->cgls", query_blocks, key_blocks, precision=precise)
    within = jnp.einsum("cgls,cgrls,csgrp->clgrp", scores, decay_mask, weighted, precision=precise)
    to_end = jnp.exp(cumulative[..., -1:] - cumulative)
    states = jnp.einsum("clgn,cgrl,clgrp->cgrpn", key_blocks, to_end, weighted, precision=precise)
    block_totals = cumulative[..., -1]
    initial = jnp.zeros(states.shape[1:], jnp.float32)
    final, entering = lax.scan(advance, initial, (states, jnp.exp(block_totals)))
    carried = jnp.einsum(
        "clgn,cgrpn,cgrl->clgrp", query_blocks, entering, jnp.exp(cumulative), precision=precise
    )
    from_start = (jnp.cumsum(block_totals, axis=0) - block_totals)[..., None] + cumulative
    return (within + carried, final, from_start, jnp.sum(block_totals, axis=0))


def normalize(rows, gain):
    widened = rows.astype(jnp.float32)
    scaled = widened * lax.rsqrt(jnp.mean(widened * widened, axis=-1, keepdims=True) + epsilon)
    return (scaled * gain).astype(jnp.bfloat16)


def per_device(
    skip_stream_entering,
    content_signal_matrix,
    writer_signal_matrix,
    reader_signal_matrix,
    multiplier_signal,
    interval_before_softplus,
    extra_log_shrink,
    log_forget_speed,
    content_filter_coefs,
    writer_filter_coefs,
    reader_filter_coefs,
    skip_path_factor,
    cluster_scaling_vector,
    blend_result_matrix,
    feature_blend_scaling,
    widening_matrix,
    narrowing_matrix,
):
    up_part = lax.all_to_all(widening_matrix, "sb", split_axis=1, concat_axis=0, tiled=True)
    narrowing_matrix, up_part = lax.optimization_barrier((narrowing_matrix, up_part))
    up_use = lax.all_gather(up_part, "sa", axis=0, tiled=True)
    down_part = lax.all_to_all(narrowing_matrix, "sb", split_axis=0, concat_axis=1, tiled=True)
    (
        content_signal_matrix,
        writer_signal_matrix,
        reader_signal_matrix,
        interval_before_softplus,
        down_part,
    ) = lax.optimization_barrier(
        (
            content_signal_matrix,
            writer_signal_matrix,
            reader_signal_matrix,
            interval_before_softplus,
            down_part,
        )
    )
    down_use = lax.all_gather(down_part, "sa")
    rim_width = content_filter_coefs.shape[0] - 1
    length = content_signal_matrix.shape[0]
    signals = (content_signal_matrix, writer_signal_matrix, reader_signal_matrix)
    tails = jnp.concatenate([signal[length - rim_width :] for signal in signals], axis=1)
    rims = shifted(tails, SP, 1)
    first, second = signals[0].shape[1], signals[0].shape[1] + signals[1].shape[1]
    values = convolve(signals[0], rims[:, :first], content_filter_coefs)
    key_rows = convolve(signals[1], rims[:, first:second], writer_filter_coefs)
    query_rows = convolve(signals[2], rims[:, second:], reader_filter_coefs)
    local_heads = interval_before_softplus.shape[0]
    local_groups = writer_signal_matrix.shape[1] // STATE
    per_group = local_heads // local_groups
    interval_lengths = jax.nn.softplus(interval_before_softplus)
    log_forgetting = extra_log_shrink - jnp.exp(log_forget_speed)[:, None] * interval_lengths
    shaped = values.reshape(length, local_groups, per_group, HEAD_DIM)
    local_out, end_state, from_start, device_total = blockwise(
        shaped,
        interval_lengths.reshape(local_groups, per_group, length),
        log_forgetting.reshape(local_groups, per_group, length),
        key_rows,
        query_rows,
    )
    incoming, up_use = prefix(device_total, end_state, up_use)
    query_blocks = query_rows.reshape(length // BLOCK, BLOCK, local_groups, STATE)
    arriving = jnp.einsum(
        "clgn,grpn,cgrl->clgrp", query_blocks, incoming, jnp.exp(from_start), precision=precise
    )
    scan_out = (local_out + arriving).reshape(length, local_heads * HEAD_DIM)
    gated = (scan_out + jnp.repeat(skip_path_factor, HEAD_DIM) * values) * jax.nn.silu(
        multiplier_signal.astype(jnp.float32)
    )
    grouped = gated.reshape(length, local_groups, -1)
    grouped = grouped * lax.rsqrt(jnp.mean(grouped * grouped, axis=-1, keepdims=True) + epsilon)
    heads_out = (grouped.reshape(length, -1) * cluster_scaling_vector).astype(jnp.bfloat16)
    mixer_rows = summed_share(
        jnp.dot(heads_out, blend_result_matrix, preferred_element_type=jnp.float32).astype(
            jnp.bfloat16
        ),
        "tp",
    )
    own_rows = (skip_stream_entering.astype(jnp.float32) + mixer_rows.astype(jnp.float32)).astype(
        jnp.bfloat16
    )
    normed = normalize(own_rows, feature_blend_scaling)
    down_whole = jnp.concatenate([down_use[k] for k in range(down_use.shape[0])], axis=1)

    def mixed(rows):
        lifted = jax.nn.relu(jnp.dot(rows, up_use, preferred_element_type=jnp.float32))
        hidden = (lifted * lifted).astype(jnp.bfloat16)
        partial = jnp.dot(hidden, down_whole, preferred_element_type=jnp.float32)
        return partial.astype(jnp.bfloat16)

    if lax.axis_size("tp") == 2:
        members, width = lax.axis_size("sb"), normed.shape[1]
        swap = [(0, 1), (1, 0)]
        copies = jnp.broadcast_to(normed[None], (members,) + normed.shape)
        own_half = lax.all_to_all(copies, "sb", split_axis=0, concat_axis=0)
        own_half = own_half.reshape(-1, width)
        other_half = lax.ppermute(own_half, "tp", swap)
        arrived = lax.ppermute(mixed(other_half), "tp", swap)
        joined = mixed(own_half).astype(jnp.float32) + arrived.astype(jnp.float32)
        joined = joined.astype(jnp.bfloat16).reshape(members, -1, width)
        shares = lax.all_to_all(joined, "sb", split_axis=0, concat_axis=0)
        mlp_rows = jnp.sum(shares.astype(jnp.float32), axis=0)
    else:
        team_rows = lax.all_gather(normed, ("sb", "tp"), axis=0, tiled=True)
        mlp_rows = lax.psum_scatter(
            mixed(team_rows), ("sb", "tp"), scatter_dimension=0, tiled=True
        )
    mlp_rows = mlp_rows.astype(jnp.bfloat16)
    return (own_rows.astype(jnp.float32) + mlp_rows.astype(jnp.float32)).astype(jnp.bfloat16)


def solution(mesh):
    shards, halves = mesh.shape["sp"], mesh.shape["tp"]
    team = math.gcd(shards, TEAM)
    teams = jax.sharding.Mesh(
        mesh.devices.reshape(shards // team, team, halves), ("sa", "sb", "tp")
    )
    placed = (
        P(("sa", "sb", "tp"), None),
        P(SP, "tp"),
        P(SP, "tp"),
        P(SP, "tp"),
        P(SP, "tp"),
        P("tp", SP),
        P("tp", SP),
        P("tp"),
        P(None, "tp"),
        P(None, "tp"),
        P(None, "tp"),
        P("tp"),
        P("tp"),
        P("tp", None),
        P(),
        P(SP, "tp"),
        P("tp", SP),
    )
    return jax.shard_map(
        per_device, mesh=teams, in_specs=placed, out_specs=P(("sa", "sb", "tp"), None), check_vma=False
    )
```

profile of v0, /device:TPU:0, one launch (start us, length us, event | category | flops | bytes accessed | tf_op | source)
XLA Modules:
  0.0 260.0 jit_solution(1598236233495418701)
XLA Ops:
  6.5 1.6 copy.50
  8.2 21.0 %all_to_all.59 = bf16[128,8,512]{0,2,1:T(8,128)(2,1)S(1)} all-to-all(bf16[128,8,512]{0,2,1:T(8,128)(2,1)S(1)} %bitcast.120), channel_id=1, replica_groups=mesh['sa'=2,'sb'=8,'tp'=2] {'sb'}, dimensions={1} | all-to-all | bytes 2097152 | tf_op jit(solution)/shard_map/all_to_all | solution.py:147
  29.2 1.3 copy.51
  30.5 3.6 %all-to-all-start.1 = ((bf16[8,512,128]{2,1,0:T(8,128)(2,1)}), bf16[8,512,128]{2,1,0:T(8,128)(2,1)S(1)}, u32[]{:S(2)}, u32[]{:S(2)}) async-start(bf16[8,512,128]{2,1,0:T(8,128)(2,1)} %bitcast.3), calls=%async_computation.1 | async-start | bytes 2097152 | tf_op jit(solution)/shard_map/all_to_all | solution.py:150
  34.3 0.6 all-gather.4.cloned.1.call-update
  34.9 12.6 %all-to-all-done.1 = bf16[8,512,128]{2,1,0:T(8,128)(2,1)S(1)} async-done(((bf16[8,512,128]{2,1,0:T(8,128)(2,1)}), bf16[8,512,128]{2,1,0:T(8,128)(2,1)S(1)}, u32[]{:S(2)}, u32[]{:S(2)}) %all-to-all-start.1) | async-done | bytes 1048608 | tf_op jit(solution)/shard_map/all_to_all | solution.py:150
  47.5 1.3 copy.52
  48.9 1.1 reduce_window_sum.17
  50.1 0.2 fusion.58
  50.2 0.2 subtract_reduce_fusion
  50.8 2.4 collective-permute-start
  53.3 0.3 copy.56
  53.7 1.0 collective-permute-done
  54.7 0.3 copy.55
  55.0 2.2 divide_multiply_fusion
  57.2 0.3 divide_multiply_fusion.1
  57.7 1.1 fusion.24
  58.8 0.3 add_convert_fusion.1
  59.2 46.4 %all_to_all.60 = bf16[16,144,128]{2,1,0:T(8,128)(2,1)S(1)} all-to-all(bf16[16,144,128]{2,1,0:T(8,128)(2,1)S(1)} %pad_maximum_fusion.3), channel_id=1, replica_groups=mesh['sa'=2,'sb'=8,'tp'=2] {'sa','sb'}, dimensions={0} | all-to-all | bytes 1179648 | tf_op jit(solution)/shard_map/all_to_all | solution.py:47
  105.6 0.8 slice.151.parts
  106.5 1.3 broadcast_in_dim.32.factors
  107.8 2.3 shard_map.163
  110.1 3.8 %all-to-all-start.3 = ((bf16[16,128,128]{2,1,0:T(8,128)(2,1)}), bf16[16,128,128]{2,1,0:T(8,128)(2,1)S(1)}, u32[]{:S(2)}, u32[]{:S(2)}) async-start(bf16[16,128,128]{2,1,0:T(8,128)(2,1)} %shard_map.163), calls=%async_computation.3 | async-start | bytes 1048576 | tf_op jit(solution)/shard_map/all_to_all | solution.py:55
  114.0 0.3 copy.61
  114.4 0.7 fusion.45
  115.1 5.3 %fusion.5 = f32[1,128,4,8,64]{1,4,3,2,0:T(8,128)} fusion(f32[4,128,128]{2,1,0:T(8,128)S(1)} %fusion.45, f32[4,8,128]{2,1,0:T(8,128)S(1)} %bitcast.129, pred[128,128]{1,0:T(8,128)(4,1)S(1)} %iota_compare_fusion, f32[128,4,8,64]{0,3,2,1:T(8,128)S(1)} %bitcast.114, f32[128,4,8]{0,2,1:T(8,128)S(1)} %get-tuple-element.51), kind=kOutput, calls=%fused_computation.10 | convolution fusion | flops 404488192 | bytes 2408448 | tf_op jit(solution)/shard_map/cgls,cgrls,csgrp->clgrp/dot_general | solution.py:109
  120.4 7.7 %all-to-all-done.3 = bf16[16,128,128]{2,1,0:T(8,128)(2,1)S(1)} async-done(((bf16[16,128,128]{2,1,0:T(8,128)(2,1)}), bf16[16,128,128]{2,1,0:T(8,128)(2,1)S(1)}, u32[]{:S(2)}, u32[]{:S(2)}) %all-to-all-start.3) | async-done | bytes 524320 | tf_op jit(solution)/shard_map/all_to_all | solution.py:55
  128.1 0.6 fusion.11
  128.7 0.6 copy-done
  129.3 1.0 fusion.15
  130.3 0.4 bitcast_reduce_fusion
  130.8 0.2 copy-done.11
  131.0 0.3 fusion.23
  131.4 4.7 %convolution_convert_fusion.2 = bf16[128,2048]{1,0:T(8,128)(2,1)S(1)} fusion(bf16[128,2048]{0,1:T(8,128)(2,1)S(1)} %fusion.23, bf16[2048,2048]{1,0:T(8,128)(2,1)} %param.30), kind=kOutput, calls=%fused_computation.3 | convolution fusion | flops 1074003968 | bytes 9437184 | tf_op jit(solution)/shard_map/dot_general | solution.py:202
  136.2 1.5 collective-permute-done.1
  137.8 0.2 fusion.33
  138.1 1.6 broadcast_in_dim.34
  139.7 3.6 %all-to-all-start.4 = ((bf16[8,64,2048]{2,1,0:T(8,128)(2,1)}), bf16[8,64,2048]{2,1,0:T(8,128)(2,1)S(1)}, u32[]{:S(2)}, u32[]{:S(2)}) async-start(bf16[8,64,2048]{2,1,0:T(8,128)(2,1)} %broadcast_in_dim.34), calls=%async_computation.4 | async-start | bytes 4194304 | tf_op jit(solution)/shard_map/all_to_all | solution.py:223
  143.4 0.7 all-gather.6.cloned.1.call-update
  144.1 36.8 %all-to-all-done.4 = bf16[8,64,2048]{2,1,0:T(8,128)(2,1)S(1)} async-done(((bf16[8,64,2048]{2,1,0:T(8,128)(2,1)}), bf16[8,64,2048]{2,1,0:T(8,128)(2,1)S(1)}, u32[]{:S(2)}, u32[]{:S(2)}) %all-to-all-start.4) | async-done | bytes 2097184 | tf_op jit(solution)/shard_map/all_to_all | solution.py:223
  180.9 21.1 %all-gather.6.cloned.1.call-done = bf16[1024,1024]{0,1:T(8,128)(2,1)} async-done(((bf16[512,1024]{0,1:T(8,128)(2,1)}), bf16[1024,1024]{0,1:T(8,128)(2,1)}) %all-gather.6.cloned.1.call-update) | async-done | bytes 2097168 | tf_op jit(solution)/shard_map/all_gather | solution.py:166
  202.0 2.7 %fusion.66 = (bf16[512,1024]{0,1:T(8,128)(2,1)S(1)}, bf16[512,1024]{0,1:T(8,128)(2,1)}) fusion(bf16[1024,1024]{0,1:T(8,128)(2,1)} %all-gather.6.cloned.1.call-done), kind=kLoop, calls=%fused_computation.127 | loop fusion | bytes 4194304 | tf_op jit(solution)/shard_map/slice | solution.py:211
  204.7 6.2 %convolution_convert_fusion = bf16[512,2048]{1,0:T(8,128)(2,1)} fusion(bf16[512,1024]{0,1:T(8,128)(2,1)} %get-tuple-element.45, bf16[512,1024]{0,1:T(8,128)(2,1)S(1)} %get-tuple-element.44, bf16[512,2048]{1,0:T(8,128)(2,1)} %collective-permute-done.2, bf16[2048,512]{1,0:T(8,128)(2,1)} %all-gather.4.cloned.1.call-done), kind=kOutput, calls=%fused_computation.1 | convolution fusion | flops 2153512960 | bytes 8388608 | tf_op jit(solution)/shard_map/dot_general | solution.py:216
  210.9 4.5 %collective-permute-done.3 = bf16[512,2048]{1,0:T(8,128)(2,1)} collective-permute-done((bf16[512,2048]{1,0:T(8,128)(2,1)}, bf16[512,2048]{1,0:T(8,128)(2,1)}, u32[]{:S(2)}, u32[]{:S(2)}) %collective-permute-start.3) | collective-permute-done | bytes 2097184 | tf_op jit(solution)/shard_map/ppermute | solution.py:226
  215.4 6.2 %add_convert_fusion = bf16[512,2048]{1,0:T(8,128)(2,1)} fusion(bf16[512,2048]{1,0:T(8,128)(2,1)} %collective-permute-done.3, bf16[512,1024]{0,1:T(8,128)(2,1)} %get-tuple-element.45, bf16[512,1024]{0,1:T(8,128)(2,1)S(1)} %get-tuple-element.44, bf16[512,2048]{1,0:T(8,128)(2,1)S(1)} %bitcast.125, bf16[2048,512]{1,0:T(8,128)(2,1)} %all-gather.4.cloned.1.call-done), kind=kOutput, calls=%fused_computation | convolution fusion | flops 2157707264 | bytes 10485760 | tf_op jit(solution)/shard_map/dot_general | solution.py:216
  221.6 30.4 %all_to_all.61 = bf16[8,64,2048]{2,1,0:T(8,128)(2,1)S(1)} all-to-all(bf16[8,64,2048]{2,1,0:T(8,128)(2,1)} %bitcast.126), channel_id=1, replica_groups=mesh['sa'=2,'sb'=8,'tp'=2] {'sb'}, dimensions={0} | all-to-all | bytes 4194304 | tf_op jit(solution)/shard_map/all_to_all | solution.py:229
  252.0 0.4 reduce_sum.36
  252.4 0.8 fusion.36
  (68 shorter events, 1.5 us)
Async XLA Ops:
  29.2 5.0 %copy-start.14 = (f32[32]{0:T(128)S(1)}, f32[32]{0:T(128)}, u32[]{:S(2)}) copy-start(f32[32]{0:T(128)} %param.24) | copy-start | bytes 388
  29.2 5.0 %copy-start.7 = (bf16[4,512]{1,0:T(4,128)(2,1)S(1)}, bf16[4,512]{1,0:T(4,128)(2,1)}, u32[]{:S(2)}) copy-start(bf16[4,512]{1,0:T(4,128)(2,1)} %param.26) | copy-start | bytes 12292
  29.2 5.0 %copy-start.8 = (bf16[4,512]{1,0:T(4,128)(2,1)S(1)}, bf16[4,512]{1,0:T(4,128)(2,1)}, u32[]{:S(2)}) copy-start(bf16[4,512]{1,0:T(4,128)(2,1)} %param.27) | copy-start | bytes 12292
  29.2 5.1 %copy-start.6 = (bf16[4,2048]{1,0:T(4,128)(2,1)S(1)}, bf16[4,2048]{1,0:T(4,128)(2,1)}, u32[]{:S(2)}) copy-start(bf16[4,2048]{1,0:T(4,128)(2,1)} %param.25) | copy-start | bytes 49156
  30.5 17.0 %all-to-all-start.1 = ((bf16[8,512,128]{2,1,0:T(8,128)(2,1)}), bf16[8,512,128]{2,1,0:T(8,128)(2,1)S(1)}, u32[]{:S(2)}, u32[]{:S(2)}) async-start(bf16[8,512,128]{2,1,0:T(8,128)(2,1)} %bitcast.3), calls=%async_computation.1 | async-start | bytes 2097152 | tf_op jit(solution)/shard_map/all_to_all | solution.py:150
  34.1 14.8 %copy-start.9 = (f32[32,128]{1,0:T(8,128)S(1)}, f32[32,128]{1,0:T(8,128)}, u32[]{:S(2)}) copy-start(f32[32,128]{1,0:T(8,128)} %param.22) | copy-start | bytes 49156
  34.1 14.8 %copy-start.10 = (f32[32,128]{1,0:T(8,128)S(1)}, f32[32,128]{1,0:T(8,128)}, u32[]{:S(2)}) copy-start(f32[32,128]{1,0:T(8,128)} %param.23) | copy-start | bytes 49156
  34.1 16.3 %copy-start.5 = (bf16[128,512]{1,0:T(8,128)(2,1)S(1)}, bf16[128,512]{1,0:T(8,128)(2,1)}, u32[]{:S(2)}) copy-start(bf16[128,512]{1,0:T(8,128)(2,1)} %param.19) | copy-start | bytes 393220
  34.1 16.3 %copy-start.4 = (bf16[128,512]{1,0:T(8,128)(2,1)S(1)}, bf16[128,512]{1,0:T(8,128)(2,1)}, u32[]{:S(2)}) copy-start(bf16[128,512]{1,0:T(8,128)(2,1)} %param.20) | copy-start | bytes 393220
  34.1 16.3 %copy-start.1 = (bf16[128,2048]{1,0:T(8,128)(2,1)S(1)}, bf16[128,2048]{1,0:T(8,128)(2,1)}, u32[]{:S(2)}) copy-start(bf16[128,2048]{1,0:T(8,128)(2,1)} %param.18) | copy-start | bytes 1572868
  34.2 76.0 %all-gather.4.cloned.1.call-start = ((), (), s32[]{:S(2)}) async-start(), calls=%async_computation.6 | async-start | bytes 3145728 | tf_op jit(solution)/shard_map/all_gather | solution.py:149
  50.8 3.9 %collective-permute-start = (bf16[3,3072]{1,0:T(4,128)(2,1)S(1)}, bf16[3,3072]{1,0:T(4,128)(2,1)S(1)}, u32[]{:S(2)}, u32[]{:S(2)}) collective-permute-start(bf16[3,3072]{1,0:T(4,128)(2,1)S(1)} %pad_maximum_fusion.7), channel_id=1, source_target_pairs={{0,2},{2,4},{4,6},{6,8},{8,10},{10,12},{12,14},{14,16},{16,18},{18... | collective-permute-start | bytes 55304 | tf_op jit(solution)/shard_map/ppermute | solution.py:22
  106.4 7.4 %copy-start.13 = (f32[32]{0:T(128)S(1)}, f32[32]{0:T(128)}, u32[]{:S(2)}) copy-start(f32[32]{0:T(128)} %param.28) | copy-start | bytes 388
  106.5 7.6 %copy-start.2 = (bf16[128,2048]{1,0:T(8,128)(2,1)S(1)}, bf16[128,2048]{1,0:T(8,128)(2,1)}, u32[]{:S(2)}) copy-start(bf16[128,2048]{1,0:T(8,128)(2,1)} %param.21) | copy-start | bytes 1572868
  110.1 18.0 %all-to-all-start.3 = ((bf16[16,128,128]{2,1,0:T(8,128)(2,1)}), bf16[16,128,128]{2,1,0:T(8,128)(2,1)S(1)}, u32[]{:S(2)}, u32[]{:S(2)}) async-start(bf16[16,128,128]{2,1,0:T(8,128)(2,1)} %shard_map.163), calls=%async_computation.3 | async-start | bytes 1048576 | tf_op jit(solution)/shard_map/all_to_all | solution.py:55
  128.1 1.2 copy-start
  130.3 0.7 copy-start.11
  131.4 6.4 %copy-start.3 = (bf16[64,2048]{1,0:T(8,128)(2,1)S(1)}, bf16[64,2048]{1,0:T(8,128)(2,1)}, u32[]{:S(2)}) copy-start(bf16[64,2048]{1,0:T(8,128)(2,1)} %param.17) | copy-start | bytes 786436
  131.4 6.6 %copy-start.12 = (f32[2048]{0:T(1024)S(1)}, f32[2048]{0:T(1024)}, u32[]{:S(2)}) copy-start(f32[2048]{0:T(1024)} %param.31) | copy-start | bytes 24580
  136.2 1.6 collective-permute-start.1
  139.7 41.1 %all-to-all-start.4 = ((bf16[8,64,2048]{2,1,0:T(8,128)(2,1)}), bf16[8,64,2048]{2,1,0:T(8,128)(2,1)S(1)}, u32[]{:S(2)}, u32[]{:S(2)}) async-start(bf16[8,64,2048]{2,1,0:T(8,128)(2,1)} %broadcast_in_dim.34), calls=%async_computation.4 | async-start | bytes 4194304 | tf_op jit(solution)/shard_map/all_to_all | solution.py:223
  143.4 58.6 %all-gather.6.cloned.1.call-start = ((), (), s32[]{:S(2)}) async-start(), calls=%async_computation.7 | async-start | bytes 3145728 | tf_op jit(solution)/shard_map/all_gather | solution.py:166
  180.9 23.8 %collective-permute-start.2 = (bf16[512,2048]{1,0:T(8,128)(2,1)S(1)}, bf16[512,2048]{1,0:T(8,128)(2,1)}, u32[]{:S(2)}, u32[]{:S(2)}) collective-permute-start(bf16[512,2048]{1,0:T(8,128)(2,1)S(1)} %bitcast.124), channel_id=1, source_target_pairs={{0,1},{1,0},{2,3},{3,2},{4,5},{5,4},{6,7},{7,6},{8,9},{9,8},{10,11... | collective-permute-start | bytes 6291464 | tf_op jit(solution)/shard_map/ppermute | solution.py:225
  210.9 4.5 %collective-permute-start.3 = (bf16[512,2048]{1,0:T(8,128)(2,1)}, bf16[512,2048]{1,0:T(8,128)(2,1)}, u32[]{:S(2)}, u32[]{:S(2)}) collective-permute-start(bf16[512,2048]{1,0:T(8,128)(2,1)} %convolution_convert_fusion), channel_id=1, source_target_pairs={{0,1},{1,0},{2,3},{3,2},{4,5},{5,4},{6,7},{7,6},{8,9},{9,8},{10,11... | collective-permute-start | bytes 6291464 | tf_op jit(solution)/shard_map/ppermute | solution.py:226
Sparse Core Ops, SparseCore 0:
  36.5 70.7 all-gather.3
  145.7 56.1 all-gather.5
where the time goes:
time: 261 us; the launch traced here: 260 us
  blocking collectives  97.8 us (37%)
  waiting for transfers between devices  86.4 us (33%)
  matrix products  25.8 us (10%)
  between operations  13.9 us (5%)
  starting transfers between devices  13.5 us (5%)
  local copies, waits for them, and re-layouts  13.4 us (5%)
  other arithmetic  6.9 us (3%)
    all_to_all x1, blocking collectives, prefix(): packed = lax.all_to_all(packed, SP, split_axis=0, concat_axis=0)  46.4 us
    all_to_all x1, waiting for transfers between devices, per_device(): own_half = lax.all_to_all(copies, 'sb', split_axis=0, concat_axis=0)  36.8 us
    all_to_all x1, blocking collectives, per_device(): shares = lax.all_to_all(joined, 'sb', split_axis=0, concat_axis=0)  30.4 us
    all_gather x1, waiting for transfers between devices, per_device(): down_use = lax.all_gather(down_part, 'sa')  21.1 us
    all_to_all x1, blocking collectives, per_device(): lax.all_to_all(widening_matrix, 'sb', split_axis=1, concat_axis=0, tiled=...  21 us
    all_to_all x1, waiting for transfers between devices, per_device(): lax.all_to_all(narrowing_matrix, 'sb', split_axis=0, concat_axis=1, tiled...  12.6 us
    dot_general x2, matrix products, mixed(): partial = jnp.dot(hidden, down_whole, preferred_element_type=jnp.float32)  12.4 us
    all_to_all x1, waiting for transfers between devices, prefix(): lax.all_to_all(entering.reshape(rows.shape), SP, split_axis=0, concat_axi...  7.65 us
  transfers between devices with their start and end apart: 9, of which 7 were waited for; matrix products, arithmetic and copies ran while one was open for 8% of the time, Pallas kernels for 1%

commit v1 on v0

--- a/solution.py
+++ b/solution.py
@@ -1,8 +1,10 @@
+import functools
 import math
 import jax
 import jax.numpy as jnp
 from jax import lax
 from jax.experimental import pallas as pl
+from jax.experimental.pallas import tpu as pltpu
 from jax.sharding import PartitionSpec as P
 
 HEAD_DIM = 64
@@ -237,7 +239,724 @@
     return (own_rows.astype(jnp.float32) + mlp_rows.astype(jnp.float32)).astype(jnp.bfloat16)
 
 
-def solution(mesh):
+TEAM_LINKS = pl.DeviceIdType.MESH
+
+
+def split3(wide):
+    one = wide.astype(jnp.bfloat16)
+    rest = wide - one.astype(jnp.float32)
+    two = rest.astype(jnp.bfloat16)
+    return one, two, (rest - two.astype(jnp.float32)).astype(jnp.bfloat16)
+
+
+def contract(left, right, dims):
+    return lax.dot_general(left, right, (dims, ((), ())), preferred_element_type=jnp.float32)
+
+
+def exact(left, right, dims, left_split):
+    if left_split:
+        terms = [contract(part, right, dims) for part in split3(left)]
+    else:
+        terms = [contract(left, part, dims) for part in split3(right)]
+    return terms[0] + terms[1] + terms[2]
+
+
+def selector(rows, columns, per_row):
+    row = lax.broadcasted_iota(jnp.int32, (rows, columns), 0)
+    column = lax.broadcasted_iota(jnp.int32, (rows, columns), 1)
+    return jnp.where(column // per_row == row, 1.0, 0.0).astype(jnp.bfloat16)
+
+
+def layer_kernel(
+    team,
+    skip_ref,
+    content_ref,
+    writer_ref,
+    reader_ref,
+    multiplier_ref,
+    interval_ref,
+    shrink_ref,
+    speed_ref,
+    content_taps,
+    writer_taps,
+    reader_taps,
+    skip_factor,
+    cluster_gain,
+    blend_hbm,
+    feature_gain,
+    up_hbm,
+    down_hbm,
+    out_ref,
+    halo,
+    wide,
+    values,
+    value_low,
+    keyquery,
+    blend,
+    up,
+    down,
+    column_decay,
+    row_decay,
+    scan,
+    scale_in,
+    state_out,
+    state_in,
+    entering,
+    kept_decay,
+    cross_out,
+    cross_in,
+    back_out,
+    back_in,
+    heads,
+    part_out,
+    part_in,
+    state_rows,
+    acts,
+    hidden,
+    pair_out,
+    pair_in,
+    plane_out,
+    plane_in,
+    depth_out,
+    depth_in,
+    local_sem,
+    halo_ss,
+    halo_rs,
+    up_ss,
+    up_rs,
+    down_ss,
+    down_rs,
+    st_ss,
+    st_rs,
+    cr_ss,
+    cr_rs,
+    bk_ss,
+    bk_rs,
+    pt_ss,
+    pt_rs,
+    az_ss,
+    az_rs,
+    ap_ss,
+    ap_rs,
+    ad_ss,
+    ad_rs,
+    pr_ss,
+    pr_rs,
+    pl_ss,
+    pl_rs,
+    dp_ss,
+    dp_rs,
+):
+    f32, bf16 = jnp.float32, jnp.bfloat16
+    batches = plan(team)
+    shards = lax.axis_size("sp")
+    sp, tp = lax.axis_index("sp"), lax.axis_index("tp")
+    own_team, me = sp // team, lax.rem(sp, team)
+    length, inner = content_ref.shape
+    state_width = writer_ref.shape[1]
+    local_heads = interval_ref.shape[0]
+    groups = state_width // STATE
+    group_width = inner // groups
+    model = skip_ref.shape[1]
+    unit = up.shape[2]
+    slice_width = inner // team
+    half = team // 2
+    rows_own = skip_ref.shape[0]
+
+    def copy(src, dst, ss, rs, sp_to, tp_to):
+        return pltpu.make_async_remote_copy(
+            src_ref=src,
+            dst_ref=dst,
+            send_sem=ss,
+            recv_sem=rs,
+            device_id=(sp_to, tp_to),
+            device_id_type=TEAM_LINKS,
+        )
+
+    def mate(step):
+        return own_team * team + lax.rem(me + step, team)
+
+    def far(step):
+        return (1 - own_team) * team + lax.rem(me + step, team)
+
+    def flip(index, bit):
+        return index + bit - 2 * bit * lax.rem(index // bit, 2)
+
+    def weight(kind, place, target):
+        index = lax.rem(target, team)
+        offset = pl.ds(pl.multiple_of(index * unit, unit), unit)
+        if kind == 0:
+            return copy(up_hbm.at[:, offset], up.at[sp], up_ss.at[place], up_rs.at[sp], target, tp)
+        return copy(
+            down_hbm.at[offset, :], down.at[sp], down_ss.at[place], down_rs.at[sp], target, tp
+        )
+
+    def weight_near(kind, step):
+        return weight(kind, step - 1, mate(step))
+
+    def weight_far(kind, step):
+        return weight(kind, team - 1 + step, far(step))
+
+    mine = pl.ds(pl.multiple_of(me * unit, unit), unit)
+    local_up = pltpu.make_async_copy(up_hbm.at[:, mine], up.at[sp], local_sem.at[0])
+    local_down = pltpu.make_async_copy(down_hbm.at[mine, :], down.at[sp], local_sem.at[1])
+    local_blend = pltpu.make_async_copy(blend_hbm, blend, local_sem.at[2])
+    local_up.start()
+    local_down.start()
+    local_blend.start()
+
+    barrier = pltpu.get_barrier_semaphore()
+    for step in range(1, shards):
+        pl.semaphore_signal(
+            barrier,
+            inc=1,
+            device_id=(lax.rem(sp + step, shards), tp),
+            device_id_type=TEAM_LINKS,
+        )
+    pl.semaphore_signal(barrier, inc=1, device_id=(sp, 1 - tp), device_id_type=TEAM_LINKS)
+    pl.semaphore_wait(barrier, shards)
+
+    following = lax.rem(sp + 1, shards)
+    spans = ((content_ref, 0, inner), (writer_ref, inner, state_width))
+    spans = spans + ((reader_ref, inner + state_width, state_width),)
+    halo_copies = []
+    for place, (ref, first, size) in enumerate(spans):
+        halo_copies.append(
+            copy(
+                ref.at[pl.ds(length - 16, 16), :],
+                halo.at[:, pl.ds(first, size)],
+                halo_ss.at[place],
+                halo_rs.at[place],
+                following,
+                tp,
+            )
+        )
+    for one in halo_copies:
+        one.start()
+    for kind, step, where in batches[0]:
+        (weight_near if where == 0 else weight_far)(kind, step).start()
+
+    steps = interval_ref[...]
+    steps = jnp.maximum(steps, 0.0) + jnp.log1p(jnp.exp(-jnp.abs(steps)))
+    forget = shrink_ref[...] - jnp.exp(speed_ref[...]) * steps
+    row_index = lax.broadcasted_iota(jnp.int32, (length, length), 0)
+    column_index = lax.broadcasted_iota(jnp.int32, (length, length), 1)
+    lower = jnp.where(row_index >= column_index, 1.0, 0.0).astype(bf16)
+    upper = jnp.where(row_index <= column_index, 1.0, 0.0).astype(bf16)
+    unity = jnp.where(row_index == column_index, 1.0, 0.0).astype(bf16)
+    log_steps = jnp.log(steps)
+    total_rows = exact(forget, upper, ((1,), (0,)), True)
+    total_columns = exact(lower, forget, ((1,), (1,)), False)
+    log_columns = exact(unity, log_steps, ((1,), (1,)), False)
+    row_decay[...] = total_rows - log_steps
+    by_head = selector(local_heads, local_heads * length, length)
+    column_decay[...] = exact(total_columns, by_head, ((1,), (0,)), True)
+    by_channel = selector(local_heads, inner, HEAD_DIM)
+    scale_in[...] = exact(jnp.exp(total_columns), by_channel, ((1,), (0,)), True)
+    last = total_columns[length - 1 : length, :]
+    to_end = jnp.exp(last - total_columns + log_columns)
+    end_scale = exact(to_end, by_channel, ((1,), (0,)), True)
+    whole_decay = exact(
+        jnp.broadcast_to(jnp.exp(last), (16, local_heads)), by_channel, ((1,), (0,)), True
+    )
+    skip_scale = exact(
+        jnp.broadcast_to(skip_factor[...], (16, local_heads)), by_channel, ((1,), (0,)), True
+    )
+
+    for one in halo_copies:
+        one.wait_recv()
+    chunk = state_width
+    for ref, taps, first, size in (
+        (content_ref, content_taps, 0, inner),
+        (writer_ref, writer_taps, inner, state_width),
+        (reader_ref, reader_taps, inner + state_width, state_width),
+    ):
+        for start in range(0, size, chunk):
+            at = slice(start, start + chunk)
+            placed = slice(first + start, first + start + chunk)
+            wide[8:, placed] = ref[:, at].astype(f32)
+            rim = halo[:, placed].astype(f32)[8:, :]
+            wide[0:8, placed] = jnp.where(sp > 0, rim, 0.0)
+            weights = taps[:, at].astype(f32)
+            count = taps.shape[0]
+            base = 8 - (count - 1)
+            total = wide[base : base + length, placed] * weights[0:1, :]
+            for k in range(1, count):
+                total = total + wide[base + k : base + k + length, placed] * weights[k : k + 1, :]
+            total = total * (1.0 / (1.0 + jnp.exp(-total)))
+            if first == 0:
+                values[:, at] = total
+                value_low[:, at] = total.astype(bf16)
+            else:
+                keyquery[:, first - inner + start : first - inner + start + chunk] = total.astype(bf16)
+
+    weighted = (values[...] * end_scale).astype(bf16)
+    for g in range(groups):
+        keys = keyquery[:, g * STATE : (g + 1) * STATE]
+        made = contract(keys, weighted[:, g * group_width : (g + 1) * group_width], ((0,), (0,)))
+        for part in range(group_width // slice_width):
+            place = g * (group_width // slice_width) + part
+            state_out[place, 0:STATE, :] = made[
+                :, part * slice_width : (part + 1) * slice_width
+            ].astype(bf16)
+    high = whole_decay.astype(bf16)
+    low = (whole_decay - high.astype(f32)).astype(bf16)
+    first_row = lax.broadcasted_iota(jnp.int32, whole_decay.shape, 0) == 0
+    packed = jnp.where(first_row, high.astype(f32), low.astype(f32)).astype(bf16)
+    for place in range(team):
+        state_out[place, STATE : STATE + 16, :] = packed[
+            :, place * slice_width : (place + 1) * slice_width
+        ]
+    state_in[me] = state_out[me]
+    state_copies = []
+    for step in range(1, team):
+        target = mate(step)
+        state_copies.append(
+            copy(
+                state_out.at[lax.rem(target, team)],
+                state_in.at[me],
+                st_ss.at[step],
+                st_rs.at[me],
+                target,
+                tp,
+            )
+        )
+        state_copies[-1].start()
+    for kind, step, where in batches[1]:
+        (weight_near if where == 0 else weight_far)(kind, step).start()
+
+    causal = row_index >= column_index
+    causal_pair = jnp.concatenate([causal, causal], axis=1)
+    lane = lax.broadcasted_iota(jnp.int32, (length, 2 * HEAD_DIM), 1)
+    pairs_per_group = group_width // (2 * HEAD_DIM)
+    for g in range(groups):
+        keys = keyquery[:, g * STATE : (g + 1) * STATE]
+        queries = keyquery[:, state_width + g * STATE : state_width + (g + 1) * STATE]
+        scores = contract(queries, keys, ((1,), (1,)))
+        scores = jnp.concatenate([scores, scores], axis=1)
+        for j in range(pairs_per_group):
+            i = g * pairs_per_group + j
+            rows = jnp.concatenate(
+                [row_decay[2 * i : 2 * i + 1, :], row_decay[2 * i + 1 : 2 * i + 2, :]], axis=1
+            )
+            gap = column_decay[:, 2 * i * length : (2 * i + 2) * length] - rows
+            decay = jnp.exp(jnp.where(causal_pair, gap, -jnp.inf))
+            mixing = (scores * decay).astype(bf16)
+            both = values[:, i * 2 * HEAD_DIM : (i + 1) * 2 * HEAD_DIM]
+            blocks = jnp.concatenate(
+                [jnp.where(lane < HEAD_DIM, both, 0.0), jnp.where(lane < HEAD_DIM, 0.0, both)],
+                axis=0,
+            ).astype(bf16)
+            scan[:, i * 2 * HEAD_DIM : (i + 1) * 2 * HEAD_DIM] = contract(
+                mixing, blocks, ((1,), (0,))
+            )
+    scan[...] = scan[...] + skip_scale[0:1, :] * values[...]
+
+    carried = jnp.zeros((STATE, slice_width), f32)
+    kept = jnp.ones((1, slice_width), f32)
+    for step in range(1, team):
+        source = lax.rem(me + step, team)
+        copy(
+            state_in.at[source], state_in.at[source], st_ss.at[step], st_rs.at[source], sp, tp
+        ).wait_recv()
+    for place in range(team):
+        entering[place] = carried
+        kept_decay[place] = jnp.broadcast_to(kept, (8, slice_width))
+        tail = state_in[place, STATE : STATE + 16, :].astype(f32)
+        factor = tail[0:1, :] + tail[1:2, :]
+        carried = carried * factor + state_in[place, 0:STATE, :].astype(f32)
+        kept = kept * factor
+    cross_out[...] = carried.astype(bf16)
+    cross = copy(
+        cross_out, cross_in, cr_ss, cr_rs, (1 - own_team) * team + me, tp
+    )
+    cross.start()
+    for kind, step, where in batches[2]:
+        (weight_near if where == 0 else weight_far)(kind, step).start()
+    cross.wait_recv()
+    earlier = jnp.where(own_team > 0, cross_in[...].astype(f32), 0.0)
+    for place in range(team):
+        back_out[place] = (entering[place] + kept_decay[place, 0:1, :] * earlier).astype(bf16)
+    back_in[me] = back_out[me]
+    back_copies = []
+    for step in range(1, team):
+        target = mate(step)
+        back_copies.append(
+            copy(
+                back_out.at[lax.rem(target, team)],
+                back_in.at[me],
+                bk_ss.at[step],
+                bk_rs.at[me],
+                target,
+                tp,
+            )
+        )
+        back_copies[-1].start()
+    for kind, step, where in batches[3]:
+        (weight_near if where == 0 else weight_far)(kind, step).start()
+    for step in range(1, team):
+        source = lax.rem(me + step, team)
+        copy(
+            back_in.at[source], back_in.at[source], bk_ss.at[step], bk_rs.at[source], sp, tp
+        ).wait_recv()
+
+    for g in range(groups):
+        queries = keyquery[:, state_width + g * STATE : state_width + (g + 1) * STATE]
+        at = slice(g * group_width, (g + 1) * group_width)
+        per = group_width // slice_width
+        incoming = jnp.concatenate([back_in[g * per + part] for part in range(per)], axis=1)
+        arriving = contract(queries, incoming, ((1,), (0,))) * scale_in[:, at]
+        gate = multiplier_ref[:, at].astype(f32)
+        gated = (scan[:, at] + arriving) * (gate * (1.0 / (1.0 + jnp.exp(-gate))))
+        gated = gated * lax.rsqrt(jnp.mean(gated * gated, axis=1, keepdims=True) + epsilon)
+        heads[:, at] = (gated * cluster_gain[:, at]).astype(bf16)
+
+    local_blend.wait()
+    column_chunk = 512
+
+    def project(index, carry):
+        at = pl.ds(pl.multiple_of(index * column_chunk, column_chunk), column_chunk)
+        product = contract(heads[...], blend[:, at], ((1,), (0,))).astype(bf16)
+        part_out[0, :, at] = product[0:rows_own, :]
+        part_out[1, :, at] = product[rows_own:, :]
+        return carry
+
+    lax.fori_loop(0, model // column_chunk, project, 0)
+    swap = copy(part_out.at[1 - tp], part_in, pt_ss, pt_rs, sp, 1 - tp)
+    swap.start()
+    swap.wait_recv()
+    mixed = (part_out[tp].astype(f32) + part_in[...].astype(f32)).astype(bf16)
+    state = (skip_ref[...].astype(f32) + mixed.astype(f32)).astype(bf16)
+    state_rows[...] = state
+    state = state.astype(f32)
+    state = state * lax.rsqrt(jnp.mean(state * state, axis=1, keepdims=True) + epsilon)
+    acts[tp, me] = (state * feature_gain[...]).astype(bf16)
+
+    opposite = flip(me, half)
+    base = own_team * team
+    plane_first = me - lax.rem(me, half)
+    in_plane = [plane_first + lax.rem(me + k, half) for k in range(half)]
+    far_plane = [flip(index, half) for index in in_plane]
+    deep = copy(acts.at[tp, me], acts.at[tp, me], az_ss, az_rs, base + opposite, tp)
+    deep.start()
+    near_copies = []
+    for k in range(1, half):
+        near_copies.append(
+            copy(acts.at[tp, me], acts.at[tp, me], ap_ss.at[k], ap_rs.at[me], base + in_plane[k], tp)
+        )
+        near_copies[-1].start()
+    side_copies = [copy(acts.at[tp, me], acts.at[tp, me], ad_ss.at[me], ad_rs.at[me], sp, 1 - tp)]
+    side_copies[-1].start()
+    for kind, step, where in batches[4]:
+        (weight_near if where == 0 else weight_far)(kind, step).start()
+
+    def arrived(place, sems):
+        return copy(acts.at[tp, place], acts.at[tp, place], az_ss, sems, sp, tp)
+
+    arrived(opposite, az_rs).wait_recv()
+    for k in range(1, half):
+        near_copies.append(
+            copy(
+                acts.at[tp, opposite],
+                acts.at[tp, opposite],
+                ap_ss.at[half + k],
+                ap_rs.at[opposite],
+                base + in_plane[k],
+                tp,
+            )
+        )
+        near_copies[-1].start()
+    side_copies.append(
+        copy(acts.at[tp, opposite], acts.at[tp, opposite], ad_ss.at[opposite], ad_rs.at[opposite], sp, 1 - tp)
+    )
+    side_copies[-1].start()
+    for kind, step, where in batches[5]:
+        (weight_near if where == 0 else weight_far)(kind, step).start()
+    for k in range(1, half):
+        for place in (in_plane[k], far_plane[k]):
+            arrived(place, ap_rs.at[place]).wait_recv()
+            side_copies.append(
+                copy(acts.at[tp, place], acts.at[tp, place], ad_ss.at[place], ad_rs.at[place], sp, 1 - tp)
+            )
+            side_copies[-1].start()
+    for place in range(team):
+        copy(
+            acts.at[1 - tp, place], acts.at[1 - tp, place], ad_ss.at[place], ad_rs.at[place], sp, 1 - tp
+        ).wait_recv()
+
+    local_up.wait()
+    for step in range(1, shards):
+        source = lax.rem(sp + step, shards)
+        copy(up.at[source], up.at[source], up_ss.at[step - 1], up_rs.at[source], sp, tp).wait_recv()
+    up_whole = (shards * up.shape[1], unit)
+
+    def lift(index, carry):
+        core, block = index // 4, lax.rem(index, 4)
+        count = team // 4
+        rows = acts[core, pl.ds(block * count, count)].reshape(count * rows_own, model)
+        lifted = jnp.maximum(contract(rows, up[...].reshape(up_whole), ((1,), (0,))), 0.0)
+        at = pl.ds(pl.multiple_of(block * count * rows_own, count * rows_own), count * rows_own)
+        hidden[core, at, :] = (lifted * lifted).astype(bf16)
+        return carry
+
+    lax.fori_loop(0, 8, lift, 0)
+
+    local_down.wait()
+    lanes = down.shape[2]
+
+    def pair_sources(t):
+        first = lax.rem(2 * t + own_team * team, shards)
+        return first, first + 1
+
+    def pair_copy(t):
+        return copy(pair_out.at[t], pair_in.at[t], pr_ss.at[t], pr_rs.at[t], sp, 1 - tp)
+
+    def plane_copy(t, k):
+        return copy(
+            plane_out.at[t, pl.ds(0, 2), in_plane_slot(k)],
+            plane_in.at[t, k],
+            pl_ss.at[t, k],
+            pl_rs.at[t, k],
+            base + in_plane[k],
+            tp,
+        )
+
+    def in_plane_slot(k):
+        return lax.rem(me + k, half)
+
+    def depth_copy(t):
+        return copy(depth_out.at[t], depth_in.at[t], dp_ss.at[t], dp_rs.at[t], base + opposite, tp)
+
+    def lower_step(t):
+        sources = pair_sources(t)
+        for source in sources:
+
+            @pl.when(source != sp)
+            def _():
+                copy(
+                    down.at[source], down.at[source], down_ss.at[0], down_rs.at[source], sp, tp
+                ).wait_recv()
+
+        both = jnp.concatenate([down[sources[0]], down[sources[1]]], axis=1)
+        pair_out[t] = contract(hidden[1 - tp], both, ((1,), (0,))).astype(bf16)
+        pair_copy(t).start()
+        plane_sum = contract(hidden[tp], both, ((1,), (0,)))
+        plane_out[t] = plane_sum.astype(bf16).reshape(2, half, rows_own, 2 * lanes)
+
+    def pair_step(t):
+        pair_copy(t).wait_recv()
+        summed = plane_out[t].astype(f32) + pair_in[t].reshape(
+            2, half, rows_own, 2 * lanes
+        ).astype(f32)
+        plane_out[t] = summed.astype(bf16)
+        for k in range(1, half):
+            plane_copy(t, k).start()
+
+    def plane_step(t):
+        summed = plane_out[t, :, lax.rem(me, half)].astype(f32)
+        for k in range(1, half):
+            plane_copy(t, k).wait_recv()
+            summed = summed + plane_in[t, k].astype(f32)
+        side = me // half
+        plane_out[t, :, lax.rem(me, half)] = summed.astype(bf16)
+        depth_out[t] = plane_out[t, 1 - side, lax.rem(me, half)]
+        depth_copy(t).start()
+
+    def depth_step(t):
+        depth_copy(t).wait_recv()
+        side = me // half
+        summed = plane_out[t, side, lax.rem(me, half)].astype(f32) + depth_in[t].astype(f32)
+        summed = summed.astype(bf16).astype(f32)
+        for place, source in enumerate(pair_sources(t)):
+            at = pl.ds(pl.multiple_of(source * lanes, lanes), lanes)
+            total = state_rows[:, at].astype(f32) + summed[:, place * lanes : (place + 1) * lanes]
+            out_ref[:, at] = total.astype(bf16)
+
+    count = shards // 2
+
+    def stage(t, carry):
+        @pl.when(t < count)
+        def _():
+            lower_step(t)
+
+        @pl.when((t >= 1) & (t < count + 1))
+        def _():
+            pair_step(t - 1)
+
+        @pl.when((t >= 2) & (t < count + 2))
+        def _():
+            plane_step(t - 2)
+
+        @pl.when(t >= 3)
+        def _():
+            depth_step(t - 3)
+
+        return carry
+
+    lax.fori_loop(0, count + 3, stage, 0)
+
+    for one in halo_copies + state_copies + back_copies + near_copies + side_copies:
+        one.wait_send()
+    for one in (cross, swap, deep):
+        one.wait_send()
+    for kind in range(2):
+        for step in range(1, team):
+            weight_near(kind, step).wait_send()
+        for step in range(team):
+            weight_far(kind, step).wait_send()
+
+    def drain(t, carry):
+        pair_copy(t).wait_send()
+        depth_copy(t).wait_send()
+        for k in range(1, half):
+            plane_copy(t, k).wait_send()
+        return carry
+
+    lax.fori_loop(0, count, drain, 0)
+
+
+def plan(team):
+    ups_far = [(0, step, 1) for step in range(team)]
+    downs_far = [(1, step, 1) for step in range(team)]
+    ups_near = [(0, step, 0) for step in range(1, team)]
+    downs_near = [(1, step, 0) for step in range(1, team)]
+    a, b = team // 4, team // 2
+    return (
+        ups_far[:a] + ups_near[:a],
+        ups_far[a : 2 * a] + ups_near[a : 2 * a],
+        ups_far[2 * a : 2 * a + 1] + ups_near[2 * a : 2 * a + 1],
+        ups_far[2 * a + 1 : 3 * a] + ups_near[2 * a + 1 : 3 * a],
+        ups_far[3 * a :] + ups_near[3 * a :],
+        downs_near + downs_far,
+    )
+
+
+def per_device_fused(team, *operands):
+    (
+        skip_stream_entering,
+        content_signal_matrix,
+        writer_signal_matrix,
+        reader_signal_matrix,
+        multiplier_signal,
+        interval_before_softplus,
+        extra_log_shrink,
+        log_forget_speed,
+        content_filter_coefs,
+        writer_filter_coefs,
+        reader_filter_coefs,
+        skip_path_factor,
+        cluster_scaling_vector,
+        blend_result_matrix,
+        feature_blend_scaling,
+        widening_matrix,
+        narrowing_matrix,
+    ) = operands
+    f32, bf16 = jnp.float32, jnp.bfloat16
+    shards = lax.axis_size("sp")
+    length, inner = content_signal_matrix.shape
+    state_width = writer_signal_matrix.shape[1]
+    local_heads = interval_before_softplus.shape[0]
+    rows_own, model = skip_stream_entering.shape
+    unit = widening_matrix.shape[1] // team
+    depth = widening_matrix.shape[0]
+    lanes = narrowing_matrix.shape[1]
+    slice_width = inner // team
+    half, pairs = team // 2, shards // 2
+    dma = pltpu.SemaphoreType.DMA
+    vmem, anywhere = pl.BlockSpec(memory_space=pltpu.VMEM), pl.BlockSpec(memory_space=pl.ANY)
+    specs = [vmem] * 13 + [anywhere, vmem, anywhere, anywhere]
+    scratch = [
+        pltpu.VMEM((16, inner + 2 * state_width), bf16),
+        pltpu.VMEM((8 + length, inner + 2 * state_width), f32),
+        pltpu.VMEM((length, inner), f32),
+        pltpu.VMEM((length, inner), bf16),
+        pltpu.VMEM((length, 2 * state_width), bf16),
+        pltpu.VMEM(blend_result_matrix.shape, bf16),
+        pltpu.VMEM((shards, depth, unit), bf16),
+        pltpu.VMEM((shards, unit, lanes), bf16),
+        pltpu.VMEM((length, local_heads * length), f32),
+        pltpu.VMEM((local_heads, length), f32),
+        pltpu.VMEM((length, inner), f32),
+        pltpu.VMEM((length, inner), f32),
+        pltpu.VMEM((team, STATE + 16, slice_width), bf16),
+        pltpu.VMEM((team, STATE + 16, slice_width), bf16),
+        pltpu.VMEM((team, STATE, slice_width), f32),
+        pltpu.VMEM((team, 8, slice_width), f32),
+        pltpu.VMEM((STATE, slice_width), bf16),
+        pltpu.VMEM((STATE, slice_width), bf16),
+        pltpu.VMEM((team, STATE, slice_width), bf16),
+        pltpu.VMEM((team, STATE, slice_width), bf16),
+        pltpu.VMEM((length, inner), bf16),
+        pltpu.VMEM((2, rows_own, model), bf16),
+        pltpu.VMEM((rows_own, model), bf16),
+        pltpu.VMEM((rows_own, model), bf16),
+        pltpu.VMEM((2, team, rows_own, model), bf16),
+        pltpu.VMEM((2, team * rows_own, unit), bf16),
+        pltpu.VMEM((pairs, team * rows_own, 2 * lanes), bf16),
+        pltpu.VMEM((pairs, team * rows_own, 2 * lanes), bf16),
+        pltpu.VMEM((pairs, 2, half, rows_own, 2 * lanes), bf16),
+        pltpu.VMEM((pairs, half, 2, rows_own, 2 * lanes), bf16),
+        pltpu.VMEM((pairs, rows_own, 2 * lanes), bf16),
+        pltpu.VMEM((pairs, rows_own, 2 * lanes), bf16),
+        dma((3,)),
+        dma((3,)),
+        dma((3,)),
+        dma((shards,)),
+        dma((shards,)),
+        dma((shards,)),
+        dma((shards,)),
+        dma((team,)),
+        dma((team,)),
+        dma,
+        dma,
+        dma((team,)),
+        dma((team,)),
+        dma,
+        dma,
+        dma,
+        dma,
+        dma((team,)),
+        dma((team,)),
+        dma((team,)),
+        dma((team,)),
+        dma((pairs,)),
+        dma((pairs,)),
+        dma((pairs, half)),
+        dma((pairs, half)),
+        dma((pairs,)),
+        dma((pairs,)),
+    ]
+    return pl.pallas_call(
+        functools.partial(layer_kernel, team),
+        out_shape=jax.ShapeDtypeStruct((rows_own, model), bf16),
+        in_specs=specs,
+        out_specs=vmem,
+        scratch_shapes=scratch,
+        compiler_params=pltpu.CompilerParams(
+            collective_id=0, has_side_effects=True, vmem_limit_bytes=63 * 1024 * 1024
+        ),
+    )(
+        skip_stream_entering,
+        content_signal_matrix,
+        writer_signal_matrix,
+        reader_signal_matrix,
+        multiplier_signal,
+        interval_before_softplus,
+        extra_log_shrink,
+        log_forget_speed.reshape(-1, 1),
+        content_filter_coefs,
+        writer_filter_coefs,
+        reader_filter_coefs,
+        skip_path_factor.reshape(1, -1),
+        cluster_scaling_vector.reshape(1, -1),
+        blend_result_matrix,
+        feature_blend_scaling.reshape(1, -1),
+        widening_matrix,
+        narrowing_matrix,
+    )
+
+
+def general_solution(mesh):
     shards, halves = mesh.shape["sp"], mesh.shape["tp"]
     team = math.gcd(shards, TEAM)
     teams = jax.sharding.Mesh(
@@ -265,3 +984,49 @@
     return jax.shard_map(
         per_device, mesh=teams, in_specs=placed, out_specs=P(("sa", "sb", "tp"), None), check_vma=False
     )
+
+
+def fits(shards, halves, team, rows, tokens, inner, hidden, model, state_width):
+    length = tokens // shards
+    local = inner // halves
+    return (
+        halves == 2
+        and shards == 2 * team
+        and team % 4 == 0
+        and length == BLOCK
+        and length % 32 == 0
+        and local % (team * 128) == 0
+        and (hidden // halves) % (team * 128) == 0
+        and model % (shards * 128) == 0
+        and (state_width // halves) % STATE == 0
+        and (local // (state_width // halves // STATE)) % (local // team) == 0
+    )
+
+
+def solution(mesh):
+    shards, halves = mesh.shape["sp"], mesh.shape["tp"]
+    team = math.gcd(shards, TEAM)
+    general = general_solution(mesh)
+    row, both = P("sp", "tp"), P(("sp", "tp"), None)
+    tp_first, tp_last, tp_only = P("tp", "sp"), P(None, "tp"), P("tp")
+    placed = (
+        (both, row, row, row, row, tp_first, tp_first, tp_only, tp_last, tp_last, tp_last)
+        + (tp_only, tp_only, P("tp", None), P(), row, tp_first)
+    )
+    fused = jax.shard_map(
+        functools.partial(per_device_fused, team),
+        mesh=mesh,
+        in_specs=placed,
+        out_specs=both,
+        check_vma=False,
+    )
+
+    def layer(*operands):
+        tokens, inner = operands[1].shape
+        model, hidden = operands[15].shape
+        state_width = operands[2].shape[1]
+        if fits(shards, halves, team, tokens, tokens, inner, hidden, model, state_width):
+            return fused(*operands)
+        return general(*operands)
+
+    return layer

time: 261 us -> 156 us (0.60)
  Pallas kernels: 2.34 us -> 152 us
  blocking collectives: 97.8 us -> 0 us
  waiting for transfers between devices: 86.4 us -> 0 us
  matrix products: 25.8 us -> 0 us
  between operations: 13.9 us -> 0.01 us
  starting transfers between devices: 13.5 us -> 0 us
  local copies, waits for them, and re-layouts: 13.4 us -> 3.01 us
  other arithmetic: 6.9 us -> 0 us
    pallas_call x1, Pallas kernels: 2.34 us -> 152 us  [per_device_fused(): pl.pallas_call(functools.partial(layer_kernel, team), out_shape=jax.Shape...]
    all_to_all x3 -> x0, blocking collectives: 97.8 us -> none  [the longest x1 46.4 us: prefix(): packed = lax.all_to_all(packed, SP, split_axis=0, concat_axis=0)]
    all_to_all x3 -> x0, waiting for transfers between devices: 57.1 us -> none  [the longest x1 36.8 us: per_device(): own_half = lax.all_to_all(copies, 'sb', split_axis=0, concat_axis=0)]
    dot_general x8 -> x0, matrix products: 25.8 us -> none  [the longest x2 12.4 us: mixed(): partial = jnp.dot(hidden, down_whole, preferred_element_type=jnp.float32)]
    all_gather x2 -> x0, waiting for transfers between devices: 21.1 us -> none  [the longest x1 21.1 us: per_device(): down_use = lax.all_gather(down_part, 'sa')]
    all_to_all x3 -> x0, starting transfers between devices: 10.9 us -> none  [the longest x1 3.75 us: prefix(): lax.all_to_all(entering.reshape(rows.shape), SP, split_axis=0, concat_axi...]
    ppermute x4 -> x0, waiting for transfers between devices: 6.98 us -> none  [the longest x1 4.5 us: per_device(): arrived = lax.ppermute(mixed(other_half), 'tp', swap)]
    slice x9 -> x0, local copies, waits for them, and re-layouts: 3.94 us -> none  [the longest x1 2.74 us: per_device(): down_use[k]]
  transfers between devices with their start and end apart: 9 -> 0, of which waited for: 7 -> 0; matrix products, arithmetic and copies ran while one was open for 8% -> 0% of each run, Pallas kernels for 1% -> 0%
where the time goes in v1:
time: 156 us; the launch traced here: 155 us
  Pallas kernels  152 us (97%)
  local copies, waits for them, and re-layouts  3.01 us (2%)
    pallas_call x1, Pallas kernels, per_device_fused(): pl.pallas_call(functools.partial(layer_kernel, team), out_shape=jax.Shape...  152 us

profile of v1, /device:TPU:0, one launch (start us, length us, event | category | flops | bytes accessed | tf_op | source)
XLA Modules:
  0.0 155.4 jit_solution(12952720418277433986)
XLA Ops:
  0.0 1.3 copy.18.speed_ref
  1.3 152.3 %shard_map.163 = bf16[64,2048]{1,0:T(8,128)(2,1)} custom-call(bf16[64,2048]{1,0:T(8,128)(2,1)} %skip_ref.1, bf16[128,2048]{1,0:T(8,128)(2,1)} %content_ref.1, bf16[128,512]{1,0:T(8,128)(2,1)} %writer_ref.1, bf16[128,512]{1,0:T(8,128)(2,1)} %reader_ref.1, bf16[128,2048]{1,0:T(8,128)(2,1)} %multiplier_ref.1, f32[32,128]{1,0:T(8,128)} %interval_ref.1, ...), custom_call_target="tpu_custom_call" | custom-call | tf_op jit(solution)/shard_map/pallas_call | solution.py:929
  153.7 1.7 %copy.20 = bf16[64,2048]{1,0:T(8,128)(2,1)} copy(bf16[64,2048]{1,0:T(8,128)(2,1)} %shard_map.163) | data formatting | bytes 524288

commit v2 on v1

--- a/solution.py
+++ b/solution.py
@@ -290,7 +290,6 @@
     halo,
     wide,
     values,
-    value_low,
     keyquery,
     blend,
     up,
@@ -316,8 +315,6 @@
     pair_out,
     pair_in,
     plane_out,
-    plane_in,
-    depth_out,
     depth_in,
     local_sem,
     halo_ss,
@@ -334,21 +331,17 @@
     bk_rs,
     pt_ss,
     pt_rs,
-    az_ss,
-    az_rs,
     ap_ss,
     ap_rs,
     ad_ss,
     ad_rs,
     pr_ss,
     pr_rs,
-    pl_ss,
-    pl_rs,
     dp_ss,
     dp_rs,
 ):
     f32, bf16 = jnp.float32, jnp.bfloat16
-    batches = plan(team)
+    batches = plan(lax.axis_size("sp") // 4)
     shards = lax.axis_size("sp")
     sp, tp = lax.axis_index("sp"), lax.axis_index("tp")
     own_team, me = sp // team, lax.rem(sp, team)
@@ -363,6 +356,15 @@
     half = team // 2
     rows_own = skip_ref.shape[0]
 
+    open_scope = []
+
+    def phase(name):
+        if open_scope:
+            open_scope.pop().__exit__(None, None, None)
+        if name:
+            open_scope.append(jax.named_scope(name))
+            open_scope[-1].__enter__()
+
     def copy(src, dst, ss, rs, sp_to, tp_to):
         return pltpu.make_async_remote_copy(
             src_ref=src,
@@ -376,30 +378,59 @@
     def mate(step):
         return own_team * team + lax.rem(me + step, team)
 
-    def far(step):
-        return (1 - own_team) * team + lax.rem(me + step, team)
-
-    def flip(index, bit):
-        return index + bit - 2 * bit * lax.rem(index // bit, 2)
-
-    def weight(kind, place, target):
-        index = lax.rem(target, team)
+    level, spot = sp // 4, lax.rem(sp, 4)
+    beside = (spot + 1 - 2 * lax.rem(spot, 2), lax.rem(spot + 2, 4))
+    levels = shards // 4
+
+    def level_at(step):
+        return lax.rem(level + levels + step, levels)
+
+    def weight_piece(kind, index):
         offset = pl.ds(pl.multiple_of(index * unit, unit), unit)
-        if kind == 0:
-            return copy(up_hbm.at[:, offset], up.at[sp], up_ss.at[place], up_rs.at[sp], target, tp)
-        return copy(
-            down_hbm.at[offset, :], down.at[sp], down_ss.at[place], down_rs.at[sp], target, tp
-        )
-
-    def weight_near(kind, step):
-        return weight(kind, step - 1, mate(step))
-
-    def weight_far(kind, step):
-        return weight(kind, team - 1 + step, far(step))
-
-    mine = pl.ds(pl.multiple_of(me * unit, unit), unit)
-    local_up = pltpu.make_async_copy(up_hbm.at[:, mine], up.at[sp], local_sem.at[0])
-    local_down = pltpu.make_async_copy(down_hbm.at[mine, :], down.at[sp], local_sem.at[1])
+        return up_hbm.at[:, offset] if kind == 0 else down_hbm.at[offset, :]
+
+    def weight_copy(kind, src, source, place, target):
+        into, ss, rs = ((up, up_ss, up_rs), (down, down_ss, down_rs))[kind]
+        if src is None:
+            src = into.at[source]
+        return copy(src, into.at[source], ss.at[place], rs.at[source], target, tp)
+
+    def source_level(step):
+        if step == 0:
+            return level
+        return step - 1 + jnp.where(level <= step - 1, 1, 0)
+
+    def rise(kind, step):
+        to = level_at(step)
+        return weight_copy(kind, weight_piece(kind, to), sp, step, to * 4 + spot)
+
+    def first_pass(kind, step):
+        source = source_level(step) * 4 + spot
+        piece = weight_piece(kind, level) if step == 0 else None
+        return weight_copy(kind, piece, source, 4 + step, level * 4 + beside[kind])
+
+    def second_pass(kind, step, other):
+        source = source_level(step) * 4 + (beside[kind] if other else spot)
+        piece = weight_piece(kind, level) if step == 0 and not other else None
+        place = 8 + step + (4 if other else 0)
+        return weight_copy(kind, piece, source, place, level * 4 + beside[1 - kind])
+
+    def issue(batch):
+        for what, kind, step in batches.get(batch, ()):
+            if what == "rise":
+                rise(kind, step).start()
+            if what == "first":
+                if step:
+                    first_pass(kind, step).wait_recv()
+                first_pass(kind, step).start()
+            if what == "own":
+                second_pass(kind, step, False).start()
+            if what == "other":
+                second_pass(kind, step, True).wait_recv()
+                second_pass(kind, step, True).start()
+
+    local_up = pltpu.make_async_copy(weight_piece(0, level), up.at[sp], local_sem.at[0])
+    local_down = pltpu.make_async_copy(weight_piece(1, level), down.at[sp], local_sem.at[1])
     local_blend = pltpu.make_async_copy(blend_hbm, blend, local_sem.at[2])
     local_up.start()
     local_down.start()
@@ -414,31 +445,14 @@
             device_id_type=TEAM_LINKS,
         )
     pl.semaphore_signal(barrier, inc=1, device_id=(sp, 1 - tp), device_id_type=TEAM_LINKS)
-    pl.semaphore_wait(barrier, shards)
-
-    following = lax.rem(sp + 1, shards)
-    spans = ((content_ref, 0, inner), (writer_ref, inner, state_width))
-    spans = spans + ((reader_ref, inner + state_width, state_width),)
-    halo_copies = []
-    for place, (ref, first, size) in enumerate(spans):
-        halo_copies.append(
-            copy(
-                ref.at[pl.ds(length - 16, 16), :],
-                halo.at[:, pl.ds(first, size)],
-                halo_ss.at[place],
-                halo_rs.at[place],
-                following,
-                tp,
-            )
-        )
-    for one in halo_copies:
-        one.start()
-    for kind, step, where in batches[0]:
-        (weight_near if where == 0 else weight_far)(kind, step).start()
-
+
+    phase("decays")
     steps = interval_ref[...]
     steps = jnp.maximum(steps, 0.0) + jnp.log1p(jnp.exp(-jnp.abs(steps)))
-    forget = shrink_ref[...] - jnp.exp(speed_ref[...]) * steps
+    head_row = lax.broadcasted_iota(jnp.int32, (local_heads, local_heads), 0)
+    head_column = lax.broadcasted_iota(jnp.int32, (local_heads, local_heads), 1)
+    speed = jnp.where(head_row == head_column, speed_ref[...], 0.0)
+    forget = shrink_ref[...] - jnp.exp(jnp.sum(speed, axis=1, keepdims=True)) * steps
     row_index = lax.broadcasted_iota(jnp.int32, (length, length), 0)
     column_index = lax.broadcasted_iota(jnp.int32, (length, length), 1)
     lower = jnp.where(row_index >= column_index, 1.0, 0.0).astype(bf16)
@@ -463,8 +477,43 @@
         jnp.broadcast_to(skip_factor[...], (16, local_heads)), by_channel, ((1,), (0,)), True
     )
 
-    for one in halo_copies:
-        one.wait_recv()
+    phase("barrier_wait")
+    pl.semaphore_wait(barrier, shards)
+    phase("first_sends")
+    following = lax.rem(sp + 1, shards)
+    spans = ((content_ref, 0, inner), (writer_ref, inner, state_width))
+    spans = spans + ((reader_ref, inner + state_width, state_width),)
+    halo_copies = []
+    for place, (ref, first, size) in enumerate(spans):
+        halo_copies.append(
+            copy(
+                ref.at[pl.ds(length - 16, 16), :],
+                halo.at[:, pl.ds(first, size)],
+                halo_ss.at[place],
+                halo_rs.at[place],
+                following,
+                tp,
+            )
+        )
+
+    @pl.when(sp < shards - 1)
+    def _():
+        for one in halo_copies:
+            one.start()
+
+    issue(0)
+
+    phase("rim_wait")
+    @pl.when(sp > 0)
+    def _():
+        for one in halo_copies:
+            one.wait_recv()
+
+    @pl.when(sp == 0)
+    def _():
+        halo[...] = jnp.zeros_like(halo)
+
+    phase("convolve")
     chunk = state_width
     for ref, taps, first, size in (
         (content_ref, content_taps, 0, inner),
@@ -475,8 +524,7 @@
             at = slice(start, start + chunk)
             placed = slice(first + start, first + start + chunk)
             wide[8:, placed] = ref[:, at].astype(f32)
-            rim = halo[:, placed].astype(f32)[8:, :]
-            wide[0:8, placed] = jnp.where(sp > 0, rim, 0.0)
+            wide[0:8, placed] = halo[:, placed].astype(f32)[8:, :]
             weights = taps[:, at].astype(f32)
             count = taps.shape[0]
             base = 8 - (count - 1)
@@ -486,10 +534,10 @@
             total = total * (1.0 / (1.0 + jnp.exp(-total)))
             if first == 0:
                 values[:, at] = total
-                value_low[:, at] = total.astype(bf16)
             else:
                 keyquery[:, first - inner + start : first - inner + start + chunk] = total.astype(bf16)
 
+    phase("states")
     weighted = (values[...] * end_scale).astype(bf16)
     for g in range(groups):
         keys = keyquery[:, g * STATE : (g + 1) * STATE]
@@ -522,9 +570,9 @@
             )
         )
         state_copies[-1].start()
-    for kind, step, where in batches[1]:
-        (weight_near if where == 0 else weight_far)(kind, step).start()
-
+    issue(1)
+
+    phase("within")
     causal = row_index >= column_index
     causal_pair = jnp.concatenate([causal, causal], axis=1)
     lane = lax.broadcasted_iota(jnp.int32, (length, 2 * HEAD_DIM), 1)
@@ -552,6 +600,7 @@
             )
     scan[...] = scan[...] + skip_scale[0:1, :] * values[...]
 
+    phase("state_wait")
     carried = jnp.zeros((STATE, slice_width), f32)
     kept = jnp.ones((1, slice_width), f32)
     for step in range(1, team):
@@ -559,6 +608,7 @@
         copy(
             state_in.at[source], state_in.at[source], st_ss.at[step], st_rs.at[source], sp, tp
         ).wait_recv()
+    phase("prefix")
     for place in range(team):
         entering[place] = carried
         kept_decay[place] = jnp.broadcast_to(kept, (8, slice_width))
@@ -567,16 +617,30 @@
         carried = carried * factor + state_in[place, 0:STATE, :].astype(f32)
         kept = kept * factor
     cross_out[...] = carried.astype(bf16)
-    cross = copy(
-        cross_out, cross_in, cr_ss, cr_rs, (1 - own_team) * team + me, tp
-    )
-    cross.start()
-    for kind, step, where in batches[2]:
-        (weight_near if where == 0 else weight_far)(kind, step).start()
-    cross.wait_recv()
-    earlier = jnp.where(own_team > 0, cross_in[...].astype(f32), 0.0)
-    for place in range(team):
-        back_out[place] = (entering[place] + kept_decay[place, 0:1, :] * earlier).astype(bf16)
+    cross = copy(cross_out, cross_in, cr_ss, cr_rs, team + me, tp)
+
+    @pl.when(own_team == 0)
+    def _():
+        cross.start()
+
+    issue(2)
+    phase("cross_wait")
+    @pl.when(own_team > 0)
+    def _():
+        cross.wait_recv()
+
+    phase("back")
+
+    @pl.when(own_team == 0)
+    def _():
+        back_out[...] = entering[...].astype(bf16)
+
+    @pl.when(own_team > 0)
+    def _():
+        earlier = cross_in[...].astype(f32)
+        for place in range(team):
+            back_out[place] = (entering[place] + kept_decay[place, 0:1, :] * earlier).astype(bf16)
+
     back_in[me] = back_out[me]
     back_copies = []
     for step in range(1, team):
@@ -592,14 +656,15 @@
             )
         )
         back_copies[-1].start()
-    for kind, step, where in batches[3]:
-        (weight_near if where == 0 else weight_far)(kind, step).start()
+    issue(3)
+    phase("back_wait")
     for step in range(1, team):
         source = lax.rem(me + step, team)
         copy(
             back_in.at[source], back_in.at[source], bk_ss.at[step], bk_rs.at[source], sp, tp
         ).wait_recv()
 
+    phase("gate")
     for g in range(groups):
         queries = keyquery[:, state_width + g * STATE : state_width + (g + 1) * STATE]
         at = slice(g * group_width, (g + 1) * group_width)
@@ -611,6 +676,7 @@
         gated = gated * lax.rsqrt(jnp.mean(gated * gated, axis=1, keepdims=True) + epsilon)
         heads[:, at] = (gated * cluster_gain[:, at]).astype(bf16)
 
+    phase("project")
     local_blend.wait()
     column_chunk = 512
 
@@ -624,148 +690,139 @@
     lax.fori_loop(0, model // column_chunk, project, 0)
     swap = copy(part_out.at[1 - tp], part_in, pt_ss, pt_rs, sp, 1 - tp)
     swap.start()
+    phase("swap_wait")
     swap.wait_recv()
+    phase("norm")
     mixed = (part_out[tp].astype(f32) + part_in[...].astype(f32)).astype(bf16)
     state = (skip_ref[...].astype(f32) + mixed.astype(f32)).astype(bf16)
     state_rows[...] = state
     state = state.astype(f32)
     state = state * lax.rsqrt(jnp.mean(state * state, axis=1, keepdims=True) + epsilon)
-    acts[tp, me] = (state * feature_gain[...]).astype(bf16)
-
-    opposite = flip(me, half)
-    base = own_team * team
-    plane_first = me - lax.rem(me, half)
-    in_plane = [plane_first + lax.rem(me + k, half) for k in range(half)]
-    far_plane = [flip(index, half) for index in in_plane]
-    deep = copy(acts.at[tp, me], acts.at[tp, me], az_ss, az_rs, base + opposite, tp)
-    deep.start()
-    near_copies = []
-    for k in range(1, half):
-        near_copies.append(
-            copy(acts.at[tp, me], acts.at[tp, me], ap_ss.at[k], ap_rs.at[me], base + in_plane[k], tp)
-        )
-        near_copies[-1].start()
-    side_copies = [copy(acts.at[tp, me], acts.at[tp, me], ad_ss.at[me], ad_rs.at[me], sp, 1 - tp)]
-    side_copies[-1].start()
-    for kind, step, where in batches[4]:
-        (weight_near if where == 0 else weight_far)(kind, step).start()
-
-    def arrived(place, sems):
-        return copy(acts.at[tp, place], acts.at[tp, place], az_ss, sems, sp, tp)
-
-    arrived(opposite, az_rs).wait_recv()
-    for k in range(1, half):
-        near_copies.append(
-            copy(
-                acts.at[tp, opposite],
-                acts.at[tp, opposite],
-                ap_ss.at[half + k],
-                ap_rs.at[opposite],
-                base + in_plane[k],
-                tp,
-            )
-        )
-        near_copies[-1].start()
-    side_copies.append(
-        copy(acts.at[tp, opposite], acts.at[tp, opposite], ad_ss.at[opposite], ad_rs.at[opposite], sp, 1 - tp)
-    )
-    side_copies[-1].start()
-    for kind, step, where in batches[5]:
-        (weight_near if where == 0 else weight_far)(kind, step).start()
-    for k in range(1, half):
-        for place in (in_plane[k], far_plane[k]):
-            arrived(place, ap_rs.at[place]).wait_recv()
-            side_copies.append(
-                copy(acts.at[tp, place], acts.at[tp, place], ad_ss.at[place], ad_rs.at[place], sp, 1 - tp)
-            )
-            side_copies[-1].start()
-    for place in range(team):
+    acts[tp, level] = (state * feature_gain[...]).astype(bf16)
+
+    phase("gather")
+    def rows_to(place, ss, rs, target, core):
+        return copy(acts.at[tp, place], acts.at[tp, place], ss, rs, target, core)
+
+    top = levels - 1
+
+    def along(place, hop, up_way):
+        to = level_at(1 if up_way else -1) * 4 + spot
+        return rows_to(place, ap_ss.at[hop + (0 if up_way else levels)], ap_rs.at[place], to, tp)
+
+    def share(place):
+        return rows_to(place, ad_ss.at[place], ad_rs.at[place], sp, 1 - tp)
+
+    def send_along(hop):
+        @pl.when((level >= hop) & (level < top))
+        def _():
+            along(level_at(-hop), hop, True).start()
+
+        @pl.when((level + hop <= top) & (level > 0))
+        def _():
+            along(level_at(hop), hop, False).start()
+
+    send_along(0)
+    share(level).start()
+    issue(4)
+    phase("line_wait")
+    for hop in range(1, levels):
+        for up_way in (True, False):
+            place = level_at(-hop if up_way else hop)
+
+            @pl.when(level >= hop if up_way else level + hop <= top)
+            def _():
+                along(place, hop, up_way).wait_recv()
+                share(place).start()
+
+                if hop < top:
+
+                    @pl.when(level < top if up_way else level > 0)
+                    def _():
+                        along(place, hop, up_way).start()
+
+        issue(3 + 10 * hop)
+    issue(5)
+    phase("side_wait")
+    for place in range(levels):
         copy(
             acts.at[1 - tp, place], acts.at[1 - tp, place], ad_ss.at[place], ad_rs.at[place], sp, 1 - tp
         ).wait_recv()
-
+    issue(6)
+
+    phase("up_wait")
     local_up.wait()
-    for step in range(1, shards):
-        source = lax.rem(sp + step, shards)
-        copy(up.at[source], up.at[source], up_ss.at[step - 1], up_rs.at[source], sp, tp).wait_recv()
+    for step in range(levels):
+        for near in range(2):
+            source = level_at(-step) * 4 + (beside[1] if near == 0 else 3 - spot)
+            weight_copy(0, None, source, 0, sp).wait_recv()
+    phase("lift")
     up_whole = (shards * up.shape[1], unit)
 
     def lift(index, carry):
-        core, block = index // 4, lax.rem(index, 4)
-        count = team // 4
+        core, block = index // 2, lax.rem(index, 2)
+        count = levels // 2
         rows = acts[core, pl.ds(block * count, count)].reshape(count * rows_own, model)
         lifted = jnp.maximum(contract(rows, up[...].reshape(up_whole), ((1,), (0,))), 0.0)
         at = pl.ds(pl.multiple_of(block * count * rows_own, count * rows_own), count * rows_own)
         hidden[core, at, :] = (lifted * lifted).astype(bf16)
         return carry
 
-    lax.fori_loop(0, 8, lift, 0)
-
+    lax.fori_loop(0, 4, lift, 0)
+    issue(7)
+
+    phase("lower")
     local_down.wait()
     lanes = down.shape[2]
 
     def pair_sources(t):
-        first = lax.rem(2 * t + own_team * team, shards)
+        row = lax.rem(t // levels + spot // 2, 2)
+        first = lax.rem(t, levels) * 4 + row * 2
         return first, first + 1
 
     def pair_copy(t):
         return copy(pair_out.at[t], pair_in.at[t], pr_ss.at[t], pr_rs.at[t], sp, 1 - tp)
 
-    def plane_copy(t, k):
+    def depth_copy(t, k):
+        to = level_at(k)
         return copy(
-            plane_out.at[t, pl.ds(0, 2), in_plane_slot(k)],
-            plane_in.at[t, k],
-            pl_ss.at[t, k],
-            pl_rs.at[t, k],
-            base + in_plane[k],
+            plane_out.at[t, to],
+            depth_in.at[t, k],
+            dp_ss.at[t, k],
+            dp_rs.at[t, k],
+            to * 4 + spot,
             tp,
         )
-
-    def in_plane_slot(k):
-        return lax.rem(me + k, half)
-
-    def depth_copy(t):
-        return copy(depth_out.at[t], depth_in.at[t], dp_ss.at[t], dp_rs.at[t], base + opposite, tp)
 
     def lower_step(t):
         sources = pair_sources(t)
         for source in sources:
-
-            @pl.when(source != sp)
+            there = lax.rem(source, 4)
+
+            @pl.when((there == beside[0]) | (there == 3 - spot))
             def _():
-                copy(
-                    down.at[source], down.at[source], down_ss.at[0], down_rs.at[source], sp, tp
-                ).wait_recv()
+                weight_copy(1, None, source, 0, sp).wait_recv()
 
         both = jnp.concatenate([down[sources[0]], down[sources[1]]], axis=1)
         pair_out[t] = contract(hidden[1 - tp], both, ((1,), (0,))).astype(bf16)
         pair_copy(t).start()
         plane_sum = contract(hidden[tp], both, ((1,), (0,)))
-        plane_out[t] = plane_sum.astype(bf16).reshape(2, half, rows_own, 2 * lanes)
+        plane_out[t] = plane_sum.astype(bf16).reshape(levels, rows_own, 2 * lanes)
 
     def pair_step(t):
         pair_copy(t).wait_recv()
         summed = plane_out[t].astype(f32) + pair_in[t].reshape(
-            2, half, rows_own, 2 * lanes
+            levels, rows_own, 2 * lanes
         ).astype(f32)
         plane_out[t] = summed.astype(bf16)
-        for k in range(1, half):
-            plane_copy(t, k).start()
-
-    def plane_step(t):
-        summed = plane_out[t, :, lax.rem(me, half)].astype(f32)
-        for k in range(1, half):
-            plane_copy(t, k).wait_recv()
-            summed = summed + plane_in[t, k].astype(f32)
-        side = me // half
-        plane_out[t, :, lax.rem(me, half)] = summed.astype(bf16)
-        depth_out[t] = plane_out[t, 1 - side, lax.rem(me, half)]
-        depth_copy(t).start()
+        for k in range(1, levels):
+            depth_copy(t, k).start()
 
     def depth_step(t):
-        depth_copy(t).wait_recv()
-        side = me // half
-        summed = plane_out[t, side, lax.rem(me, half)].astype(f32) + depth_in[t].astype(f32)
+        summed = plane_out[t, level].astype(f32)
+        for k in range(1, levels):
+            depth_copy(t, k).wait_recv()
+            summed = summed + depth_in[t, k].astype(f32)
         summed = summed.astype(bf16).astype(f32)
         for place, source in enumerate(pair_sources(t)):
             at = pl.ds(pl.multiple_of(source * lanes, lanes), lanes)
@@ -775,60 +832,93 @@
     count = shards // 2
 
     def stage(t, carry):
+        for turn in range(levels + 1):
+            if batches.get(50 + turn):
+
+                @pl.when(t == turn)
+                def _():
+                    issue(50 + turn)
+
         @pl.when(t < count)
         def _():
-            lower_step(t)
+            with jax.named_scope("lower_step"):
+                lower_step(t)
 
         @pl.when((t >= 1) & (t < count + 1))
         def _():
-            pair_step(t - 1)
-
-        @pl.when((t >= 2) & (t < count + 2))
+            with jax.named_scope("pair_step"):
+                pair_step(t - 1)
+
+        @pl.when(t >= LAG)
         def _():
-            plane_step(t - 2)
-
-        @pl.when(t >= 3)
+            with jax.named_scope("depth_step"):
+                depth_step(t - LAG)
+
+        return carry
+
+    lax.fori_loop(0, count + LAG, stage, 0)
+
+    phase("drain")
+    @pl.when(sp < shards - 1)
+    def _():
+        for one in halo_copies:
+            one.wait_send()
+
+    for one in state_copies + back_copies:
+        one.wait_send()
+    @pl.when(own_team == 0)
+    def _():
+        cross.wait_send()
+
+    swap.wait_send()
+    for place in range(levels):
+        share(place).wait_send()
+    for hop in range(top):
+
+        @pl.when((level >= hop) & (level < top))
         def _():
-            depth_step(t - 3)
-
-        return carry
-
-    lax.fori_loop(0, count + 3, stage, 0)
-
-    for one in halo_copies + state_copies + back_copies + near_copies + side_copies:
-        one.wait_send()
-    for one in (cross, swap, deep):
-        one.wait_send()
+            along(level_at(-hop), hop, True).wait_send()
+
+        @pl.when((level + hop <= top) & (level > 0))
+        def _():
+            along(level_at(hop), hop, False).wait_send()
+
     for kind in range(2):
-        for step in range(1, team):
-            weight_near(kind, step).wait_send()
-        for step in range(team):
-            weight_far(kind, step).wait_send()
+        for step in range(levels):
+            first_pass(kind, step).wait_send()
+            second_pass(kind, step, False).wait_send()
+            second_pass(kind, step, True).wait_send()
+            if step:
+                rise(kind, step).wait_send()
 
     def drain(t, carry):
         pair_copy(t).wait_send()
-        depth_copy(t).wait_send()
-        for k in range(1, half):
-            plane_copy(t, k).wait_send()
+        for k in range(1, levels):
+            depth_copy(t, k).wait_send()
         return carry
 
     lax.fori_loop(0, count, drain, 0)
-
-
-def plan(team):
-    ups_far = [(0, step, 1) for step in range(team)]
-    downs_far = [(1, step, 1) for step in range(team)]
-    ups_near = [(0, step, 0) for step in range(1, team)]
-    downs_near = [(1, step, 0) for step in range(1, team)]
-    a, b = team // 4, team // 2
-    return (
-        ups_far[:a] + ups_near[:a],
-        ups_far[a : 2 * a] + ups_near[a : 2 * a],
-        ups_far[2 * a : 2 * a + 1] + ups_near[2 * a : 2 * a + 1],
-        ups_far[2 * a + 1 : 3 * a] + ups_near[2 * a + 1 : 3 * a],
-        ups_far[3 * a :] + ups_near[3 * a :],
-        downs_near + downs_far,
-    )
+    phase("")
+
+
+LAG = 3
+
+
+def plan(levels):
+    ur, dr = ([("rise", kind, step) for step in range(1, levels)] for kind in range(2))
+    uf, df = ([("first", kind, step) for step in range(levels)] for kind in range(2))
+    uw, dw = ([("own", kind, step) for step in range(levels)] for kind in range(2))
+    ux, dx = ([("other", kind, step) for step in range(levels)] for kind in range(2))
+    return {
+        0: ur + uf[:1] + df[:1],
+        1: uw[:1] + ux[:1] + dw[:1] + dx[:1],
+        3: dr + uf[1:] + uw[1:],
+        4: ux[1:],
+        13: df[1:] + dw[1:],
+        51: dx[1:2],
+        52: dx[2:3],
+        53: dx[3:],
+    }
 
 
 def per_device_fused(team, *operands):
@@ -857,11 +947,12 @@
     state_width = writer_signal_matrix.shape[1]
     local_heads = interval_before_softplus.shape[0]
     rows_own, model = skip_stream_entering.shape
-    unit = widening_matrix.shape[1] // team
+    levels = shards // 4
+    unit = widening_matrix.shape[1] // levels
     depth = widening_matrix.shape[0]
     lanes = narrowing_matrix.shape[1]
     slice_width = inner // team
-    half, pairs = team // 2, shards // 2
+    pairs = shards // 2
     dma = pltpu.SemaphoreType.DMA
     vmem, anywhere = pl.BlockSpec(memory_space=pltpu.VMEM), pl.BlockSpec(memory_space=pl.ANY)
     specs = [vmem] * 13 + [anywhere, vmem, anywhere, anywhere]
@@ -869,7 +960,6 @@
         pltpu.VMEM((16, inner + 2 * state_width), bf16),
         pltpu.VMEM((8 + length, inner + 2 * state_width), f32),
         pltpu.VMEM((length, inner), f32),
-        pltpu.VMEM((length, inner), bf16),
         pltpu.VMEM((length, 2 * state_width), bf16),
         pltpu.VMEM(blend_result_matrix.shape, bf16),
         pltpu.VMEM((shards, depth, unit), bf16),
@@ -890,20 +980,18 @@
         pltpu.VMEM((2, rows_own, model), bf16),
         pltpu.VMEM((rows_own, model), bf16),
         pltpu.VMEM((rows_own, model), bf16),
-        pltpu.VMEM((2, team, rows_own, model), bf16),
-        pltpu.VMEM((2, team * rows_own, unit), bf16),
-        pltpu.VMEM((pairs, team * rows_own, 2 * lanes), bf16),
-        pltpu.VMEM((pairs, team * rows_own, 2 * lanes), bf16),
-        pltpu.VMEM((pairs, 2, half, rows_own, 2 * lanes), bf16),
-        pltpu.VMEM((pairs, half, 2, rows_own, 2 * lanes), bf16),
-        pltpu.VMEM((pairs, rows_own, 2 * lanes), bf16),
-        pltpu.VMEM((pairs, rows_own, 2 * lanes), bf16),
+        pltpu.VMEM((2, levels, rows_own, model), bf16),
+        pltpu.VMEM((2, levels * rows_own, unit), bf16),
+        pltpu.VMEM((pairs, levels * rows_own, 2 * lanes), bf16),
+        pltpu.VMEM((pairs, levels * rows_own, 2 * lanes), bf16),
+        pltpu.VMEM((pairs, levels, rows_own, 2 * lanes), bf16),
+        pltpu.VMEM((pairs, levels, rows_own, 2 * lanes), bf16),
         dma((3,)),
         dma((3,)),
         dma((3,)),
+        dma((8 + 2 * levels,)),
         dma((shards,)),
-        dma((shards,)),
-        dma((shards,)),
+        dma((8 + 2 * levels,)),
         dma((shards,)),
         dma((team,)),
         dma((team,)),
@@ -913,18 +1001,14 @@
         dma((team,)),
         dma,
         dma,
-        dma,
-        dma,
-        dma((team,)),
-        dma((team,)),
-        dma((team,)),
-        dma((team,)),
+        dma((2 * levels,)),
+        dma((levels,)),
+        dma((levels,)),
+        dma((levels,)),
         dma((pairs,)),
         dma((pairs,)),
-        dma((pairs, half)),
-        dma((pairs, half)),
-        dma((pairs,)),
-        dma((pairs,)),
+        dma((pairs, levels)),
+        dma((pairs, levels)),
     ]
     return pl.pallas_call(
         functools.partial(layer_kernel, team),
@@ -943,7 +1027,7 @@
         multiplier_signal,
         interval_before_softplus,
         extra_log_shrink,
-        log_forget_speed.reshape(-1, 1),
+        log_forget_speed.reshape(1, -1),
         content_filter_coefs,
         writer_filter_coefs,
         reader_filter_coefs,
@@ -996,7 +1080,9 @@
         and length == BLOCK
         and length % 32 == 0
         and local % (team * 128) == 0
-        and (hidden // halves) % (team * 128) == 0
+        and shards % 4 == 0
+        and (hidden // halves) % (shards // 4 * 128) == 0
+        and (shards // 4) == 4
         and model % (shards * 128) == 0
         and (state_width // halves) % STATE == 0
         and (local // (state_width // halves // STATE)) % (local // team) == 0

time: 156 us -> 117 us (0.75)
  Pallas kernels: 152 us -> 116 us
    pallas_call x1, Pallas kernels: 152 us -> 116 us  [per_device_fused(): pl.pallas_call(functools.partial(layer_kernel, team), out_shape=jax.Shape...]
where the time goes in v2:
time: 117 us
  Pallas kernels  116 us (99%)
  local copies, waits for them, and re-layouts  1.67 us (1%)
    pallas_call x1, Pallas kernels, per_device_fused(): pl.pallas_call(functools.partial(layer_kernel, team), out_shape=jax.Shape...  116 us

profile of v2, /device:TPU:0, one launch (start us, length us, event | category | flops | bytes accessed | tf_op | source)
XLA Modules:
  0.0 117.2 jit_solution(9892635320072224634)
XLA Ops:
  0.0 115.5 %shard_map.163 = bf16[64,2048]{1,0:T(8,128)(2,1)} custom-call(bf16[64,2048]{1,0:T(8,128)(2,1)} %skip_ref.1, bf16[128,2048]{1,0:T(8,128)(2,1)} %content_ref.1, bf16[128,512]{1,0:T(8,128)(2,1)} %writer_ref.1, bf16[128,512]{1,0:T(8,128)(2,1)} %reader_ref.1, bf16[128,2048]{1,0:T(8,128)(2,1)} %multiplier_ref.1, f32[32,128]{1,0:T(8,128)} %interval_ref.1, ...), custom_call_target="tpu_custom_call" | custom-call | tf_op jit(solution)/shard_map/pallas_call | solution.py:1013
  115.5 1.7 %copy.19 = bf16[64,2048]{1,0:T(8,128)(2,1)} copy(bf16[64,2048]{1,0:T(8,128)(2,1)} %shard_map.163) | data formatting | bytes 524288

commit v3 on v2

--- a/solution.py
+++ b/solution.py
@@ -269,11 +269,11 @@
 
 def layer_kernel(
     team,
-    skip_ref,
-    content_ref,
-    writer_ref,
-    reader_ref,
-    multiplier_ref,
+    skip_hbm,
+    content_hbm,
+    writer_hbm,
+    reader_hbm,
+    multiplier_hbm,
     interval_ref,
     shrink_ref,
     speed_ref,
@@ -287,6 +287,11 @@
     up_hbm,
     down_hbm,
     out_ref,
+    skip_ref,
+    content_ref,
+    writer_ref,
+    reader_ref,
+    multiplier_ref,
     halo,
     wide,
     values,
@@ -323,6 +328,8 @@
     up_rs,
     down_ss,
     down_rs,
+    half_ss,
+    half_rs,
     st_ss,
     st_rs,
     cr_ss,
@@ -395,43 +402,64 @@
             src = into.at[source]
         return copy(src, into.at[source], ss.at[place], rs.at[source], target, tp)
 
-    def source_level(step):
-        if step == 0:
-            return level
+    def source_level(step, kind):
+        if kind == 0 or step == 0:
+            return level_at(-step)
         return step - 1 + jnp.where(level <= step - 1, 1, 0)
 
     def rise(kind, step):
         to = level_at(step)
         return weight_copy(kind, weight_piece(kind, to), sp, step, to * 4 + spot)
 
-    def first_pass(kind, step):
-        source = source_level(step) * 4 + spot
+    def spread(kind, step, way):
+        source = source_level(step, kind) * 4 + spot
         piece = weight_piece(kind, level) if step == 0 else None
-        return weight_copy(kind, piece, source, 4 + step, level * 4 + beside[kind])
-
-    def second_pass(kind, step, other):
-        source = source_level(step) * 4 + (beside[kind] if other else spot)
-        piece = weight_piece(kind, level) if step == 0 and not other else None
-        place = 8 + step + (4 if other else 0)
-        return weight_copy(kind, piece, source, place, level * 4 + beside[1 - kind])
+        place = levels * (1 + way) + step
+        return weight_copy(kind, piece, source, place, level * 4 + beside[way])
+
+    def relay(kind, step, way):
+        at_level = source_level(step, kind)
+        return diagonal(kind, at_level, at_level * 4 + beside[way], way, step)
+
+    def diagonal(kind, at_level, source, way, step):
+        part = pl.ds(way * (unit // 2), unit // 2)
+        held = up.at[source, :, part] if kind == 0 else down.at[source, part, :]
+        place = kind * 2 * levels + way * levels
+        target = level * 4 + beside[1 - way]
+        return copy(held, held, half_ss.at[place + step], half_rs.at[place + at_level], target, tp)
+
+    def neighbour(kind, step, way):
+        return weight_copy(kind, None, source_level(step, kind) * 4 + beside[way], 0, sp)
 
     def issue(batch):
         for what, kind, step in batches.get(batch, ()):
             if what == "rise":
                 rise(kind, step).start()
-            if what == "first":
+            if what == "spread":
                 if step:
-                    first_pass(kind, step).wait_recv()
-                first_pass(kind, step).start()
-            if what == "own":
-                second_pass(kind, step, False).start()
-            if what == "other":
-                second_pass(kind, step, True).wait_recv()
-                second_pass(kind, step, True).start()
+                    spread(kind, step, 0).wait_recv()
+                for way in range(2):
+                    spread(kind, step, way).start()
+            if what == "relay":
+                for way in range(2):
+                    neighbour(kind, step, way).wait_recv()
+                    relay(kind, step, way).start()
 
     local_up = pltpu.make_async_copy(weight_piece(0, level), up.at[sp], local_sem.at[0])
     local_down = pltpu.make_async_copy(weight_piece(1, level), down.at[sp], local_sem.at[1])
     local_blend = pltpu.make_async_copy(blend_hbm, blend, local_sem.at[2])
+    brought = []
+    for place, (source, into) in enumerate(
+        (
+            (content_hbm, content_ref),
+            (writer_hbm, writer_ref),
+            (reader_hbm, reader_ref),
+            (multiplier_hbm, multiplier_ref),
+            (skip_hbm, skip_ref),
+        )
+    ):
+        brought.append(pltpu.make_async_copy(source, into, local_sem.at[3 + place]))
+        brought[-1].start()
     local_up.start()
     local_down.start()
     local_blend.start()
@@ -477,6 +505,8 @@
         jnp.broadcast_to(skip_factor[...], (16, local_heads)), by_channel, ((1,), (0,)), True
     )
 
+    for one in brought[:3]:
+        one.wait()
     phase("barrier_wait")
     pl.semaphore_wait(barrier, shards)
     phase("first_sends")
@@ -665,6 +695,7 @@
         ).wait_recv()
 
     phase("gate")
+    brought[3].wait()
     for g in range(groups):
         queries = keyquery[:, state_width + g * STATE : state_width + (g + 1) * STATE]
         at = slice(g * group_width, (g + 1) * group_width)
@@ -693,6 +724,7 @@
     phase("swap_wait")
     swap.wait_recv()
     phase("norm")
+    brought[4].wait()
     mixed = (part_out[tp].astype(f32) + part_in[...].astype(f32)).astype(bf16)
     state = (skip_ref[...].astype(f32) + mixed.astype(f32)).astype(bf16)
     state_rows[...] = state
@@ -701,61 +733,66 @@
     acts[tp, level] = (state * feature_gain[...]).astype(bf16)
 
     phase("gather")
-    def rows_to(place, ss, rs, target, core):
-        return copy(acts.at[tp, place], acts.at[tp, place], ss, rs, target, core)
+    parts = 2
+
+    def rows_to(place, part, ss, rs, target, core):
+        rows = pl.ds(part * (rows_own // parts), rows_own // parts)
+        held = acts.at[tp, place, rows]
+        return copy(held, held, ss, rs.at[place * parts + part], target, core)
 
     top = levels - 1
 
-    def along(place, hop, up_way):
+    def along(place, part, hop, up_way):
         to = level_at(1 if up_way else -1) * 4 + spot
-        return rows_to(place, ap_ss.at[hop + (0 if up_way else levels)], ap_rs.at[place], to, tp)
-
-    def share(place):
-        return rows_to(place, ad_ss.at[place], ad_rs.at[place], sp, 1 - tp)
-
-    def send_along(hop):
+        order = (hop + (0 if up_way else levels)) * parts + part
+        return rows_to(place, part, ap_ss.at[order], ap_rs, to, tp)
+
+    def share(place, part):
+        return rows_to(place, part, ad_ss.at[place * parts + part], ad_rs, sp, 1 - tp)
+
+    def send_along(hop, part):
         @pl.when((level >= hop) & (level < top))
         def _():
-            along(level_at(-hop), hop, True).start()
+            along(level_at(-hop), part, hop, True).start()
 
         @pl.when((level + hop <= top) & (level > 0))
         def _():
-            along(level_at(hop), hop, False).start()
-
-    send_along(0)
-    share(level).start()
+            along(level_at(hop), part, hop, False).start()
+
+    for part in range(parts):
+        send_along(0, part)
+        share(level, part).start()
     issue(4)
     phase("line_wait")
     for hop in range(1, levels):
-        for up_way in (True, False):
-            place = level_at(-hop if up_way else hop)
-
-            @pl.when(level >= hop if up_way else level + hop <= top)
-            def _():
-                along(place, hop, up_way).wait_recv()
-                share(place).start()
-
-                if hop < top:
-
-                    @pl.when(level < top if up_way else level > 0)
-                    def _():
-                        along(place, hop, up_way).start()
+        for part in range(parts):
+            for up_way in (True, False):
+                place = level_at(-hop if up_way else hop)
+
+                @pl.when(level >= hop if up_way else level + hop <= top)
+                def _():
+                    along(place, part, hop, up_way).wait_recv()
+                    if hop < top:
+
+                        @pl.when(level < top if up_way else level > 0)
+                        def _():
+                            along(place, part, hop, up_way).start()
+
+                    share(place, part).start()
 
         issue(3 + 10 * hop)
     issue(5)
     phase("side_wait")
     for place in range(levels):
-        copy(
-            acts.at[1 - tp, place], acts.at[1 - tp, place], ad_ss.at[place], ad_rs.at[place], sp, 1 - tp
-        ).wait_recv()
+        for part in range(parts):
+            share(place, part).wait_recv()
     issue(6)
 
     phase("up_wait")
     local_up.wait()
     for step in range(levels):
-        for near in range(2):
-            source = level_at(-step) * 4 + (beside[1] if near == 0 else 3 - spot)
-            weight_copy(0, None, source, 0, sp).wait_recv()
+        for way in range(2):
+            diagonal(0, step, step * 4 + 3 - spot, way, 0).wait_recv()
     phase("lift")
     up_whole = (shards * up.shape[1], unit)
 
@@ -796,12 +833,12 @@
 
     def lower_step(t):
         sources = pair_sources(t)
-        for source in sources:
-            there = lax.rem(source, 4)
-
-            @pl.when((there == beside[0]) | (there == 3 - spot))
-            def _():
-                weight_copy(1, None, source, 0, sp).wait_recv()
+
+        @pl.when(t >= levels)
+        def _():
+            for way in range(2):
+                at_level = lax.rem(t, levels)
+                diagonal(1, at_level, at_level * 4 + 3 - spot, way, 0).wait_recv()
 
         both = jnp.concatenate([down[sources[0]], down[sources[1]]], axis=1)
         pair_out[t] = contract(hidden[1 - tp], both, ((1,), (0,))).astype(bf16)
@@ -816,7 +853,7 @@
         ).astype(f32)
         plane_out[t] = summed.astype(bf16)
         for k in range(1, levels):
-            depth_copy(t, k).start()
+            depth_copy(t, jnp.where(level < levels // 2, levels - k, k)).start()
 
     def depth_step(t):
         summed = plane_out[t, level].astype(f32)
@@ -871,23 +908,24 @@
         cross.wait_send()
 
     swap.wait_send()
-    for place in range(levels):
-        share(place).wait_send()
-    for hop in range(top):
-
-        @pl.when((level >= hop) & (level < top))
-        def _():
-            along(level_at(-hop), hop, True).wait_send()
-
-        @pl.when((level + hop <= top) & (level > 0))
-        def _():
-            along(level_at(hop), hop, False).wait_send()
+    for part in range(parts):
+        for place in range(levels):
+            share(place, part).wait_send()
+        for hop in range(top):
+
+            @pl.when((level >= hop) & (level < top))
+            def _():
+                along(level_at(-hop), part, hop, True).wait_send()
+
+            @pl.when((level + hop <= top) & (level > 0))
+            def _():
+                along(level_at(hop), part, hop, False).wait_send()
 
     for kind in range(2):
         for step in range(levels):
-            first_pass(kind, step).wait_send()
-            second_pass(kind, step, False).wait_send()
-            second_pass(kind, step, True).wait_send()
+            for way in range(2):
+                spread(kind, step, way).wait_send()
+                relay(kind, step, way).wait_send()
             if step:
                 rise(kind, step).wait_send()
 
@@ -906,19 +944,9 @@
 
 def plan(levels):
     ur, dr = ([("rise", kind, step) for step in range(1, levels)] for kind in range(2))
-    uf, df = ([("first", kind, step) for step in range(levels)] for kind in range(2))
-    uw, dw = ([("own", kind, step) for step in range(levels)] for kind in range(2))
-    ux, dx = ([("other", kind, step) for step in range(levels)] for kind in range(2))
-    return {
-        0: ur + uf[:1] + df[:1],
-        1: uw[:1] + ux[:1] + dw[:1] + dx[:1],
-        3: dr + uf[1:] + uw[1:],
-        4: ux[1:],
-        13: df[1:] + dw[1:],
-        51: dx[1:2],
-        52: dx[2:3],
-        53: dx[3:],
-    }
+    us, ds = ([("spread", kind, step) for step in range(levels)] for kind in range(2))
+    ut, dt = ([("relay", kind, step) for step in range(levels)] for kind in range(2))
+    return {0: [('rise', 0, 1), ('rise', 0, 2), ('spread', 0, 0)], 1: [('rise', 0, 3), ('relay', 0, 0), ('spread', 1, 0), ('spread', 0, 1)], 3: [('relay', 1, 0), ('rise', 1, 1), ('rise', 1, 2), ('rise', 1, 3), ('spread', 0, 2), ('spread', 0, 3)], 4: [('relay', 0, 1), ('relay', 0, 2), ('relay', 0, 3)], 13: [('spread', 1, 1), ('spread', 1, 2), ('spread', 1, 3)], 50: [('relay', 1, 1)], 51: [('relay', 1, 2)], 52: [('relay', 1, 3)]}
 
 
 def per_device_fused(team, *operands):
@@ -955,8 +983,13 @@
     pairs = shards // 2
     dma = pltpu.SemaphoreType.DMA
     vmem, anywhere = pl.BlockSpec(memory_space=pltpu.VMEM), pl.BlockSpec(memory_space=pl.ANY)
-    specs = [vmem] * 13 + [anywhere, vmem, anywhere, anywhere]
+    specs = [anywhere] * 5 + [vmem] * 8 + [anywhere, vmem, anywhere, anywhere]
     scratch = [
+        pltpu.VMEM((rows_own, model), bf16),
+        pltpu.VMEM((length, inner), bf16),
+        pltpu.VMEM((length, state_width), bf16),
+        pltpu.VMEM((length, state_width), bf16),
+        pltpu.VMEM((length, inner), bf16),
         pltpu.VMEM((16, inner + 2 * state_width), bf16),
         pltpu.VMEM((8 + length, inner + 2 * state_width), f32),
         pltpu.VMEM((length, inner), f32),
@@ -986,13 +1019,15 @@
         pltpu.VMEM((pairs, levels * rows_own, 2 * lanes), bf16),
         pltpu.VMEM((pairs, levels, rows_own, 2 * lanes), bf16),
         pltpu.VMEM((pairs, levels, rows_own, 2 * lanes), bf16),
+        dma((8,)),
         dma((3,)),
         dma((3,)),
-        dma((3,)),
-        dma((8 + 2 * levels,)),
+        dma((3 * levels,)),
         dma((shards,)),
-        dma((8 + 2 * levels,)),
+        dma((3 * levels,)),
         dma((shards,)),
+        dma((4 * levels,)),
+        dma((4 * levels,)),
         dma((team,)),
         dma((team,)),
         dma,
@@ -1001,10 +1036,10 @@
         dma((team,)),
         dma,
         dma,
+        dma((4 * levels,)),
         dma((2 * levels,)),
-        dma((levels,)),
-        dma((levels,)),
-        dma((levels,)),
+        dma((2 * levels,)),
+        dma((2 * levels,)),
         dma((pairs,)),
         dma((pairs,)),
         dma((pairs, levels)),

time: 117 us -> 111 us (0.949)
  Pallas kernels: 116 us -> 109 us
    pallas_call x1, Pallas kernels: 116 us -> 109 us  [per_device_fused(): pl.pallas_call(functools.partial(layer_kernel, team), out_shape=jax.Shape...]
where the time goes in v3:
time: 111 us; the launch traced here: 110 us
  Pallas kernels  109 us (98%)
  local copies, waits for them, and re-layouts  1.67 us (2%)
    pallas_call x1, Pallas kernels, per_device_fused(): pl.pallas_call(functools.partial(layer_kernel, team), out_shape=jax.Shape...  109 us

profile of v3, /device:TPU:0, one launch (start us, length us, event | category | flops | bytes accessed | tf_op | source)
XLA Modules:
  0.0 110.4 jit_solution(4540476952709822094)
XLA Ops:
  0.0 108.7 %shard_map.163 = bf16[64,2048]{1,0:T(8,128)(2,1)} custom-call(bf16[64,2048]{1,0:T(8,128)(2,1)} %skip_hbm.1, bf16[128,2048]{1,0:T(8,128)(2,1)} %content_hbm.1, bf16[128,512]{1,0:T(8,128)(2,1)} %writer_hbm.1, bf16[128,512]{1,0:T(8,128)(2,1)} %reader_hbm.1, bf16[128,2048]{1,0:T(8,128)(2,1)} %multiplier_hbm.1, f32[32,128]{1,0:T(8,128)} %interval_ref.1, ...), custom_call_target="tpu_custom_call" | custom-call | tf_op jit(solution)/shard_map/pallas_call | solution.py:1048
  108.7 1.7 %copy.19 = bf16[64,2048]{1,0:T(8,128)(2,1)} copy(bf16[64,2048]{1,0:T(8,128)(2,1)} %shard_map.163) | data formatting | bytes 524288

commit v4 on v3

--- a/solution.py
+++ b/solution.py
@@ -286,6 +286,7 @@
     feature_gain,
     up_hbm,
     down_hbm,
+    mixed_ref,
     out_ref,
     skip_ref,
     content_ref,
@@ -314,7 +315,6 @@
     heads,
     part_out,
     part_in,
-    state_rows,
     acts,
     hidden,
     pair_out,
@@ -440,6 +440,29 @@
                     spread(kind, step, 0).wait_recv()
                 for way in range(2):
                     spread(kind, step, way).start()
+            if what == "spread level":
+
+                @pl.when(level != step)
+                def _():
+                    source = step * 4 + spot
+                    slot = levels + step + jnp.where(level > step, 1, 0)
+                    for way in range(2):
+                        target = level * 4 + beside[way]
+                        passing = weight_copy(kind, None, source, slot + way * levels, target)
+                        if way == 0:
+                            passing.wait_recv()
+                        passing.start()
+
+            if what == "relay level":
+
+                @pl.when(level != step)
+                def _():
+                    slot = step + jnp.where(level > step, 1, 0)
+                    for way in range(2):
+                        source = step * 4 + beside[way]
+                        weight_copy(kind, None, source, 0, sp).wait_recv()
+                        diagonal(kind, step, source, way, slot).start()
+
             if what == "relay":
                 for way in range(2):
                     neighbour(kind, step, way).wait_recv()
@@ -727,7 +750,7 @@
     brought[4].wait()
     mixed = (part_out[tp].astype(f32) + part_in[...].astype(f32)).astype(bf16)
     state = (skip_ref[...].astype(f32) + mixed.astype(f32)).astype(bf16)
-    state_rows[...] = state
+    mixed_ref[...] = state
     state = state.astype(f32)
     state = state * lax.rsqrt(jnp.mean(state * state, axis=1, keepdims=True) + epsilon)
     acts[tp, level] = (state * feature_gain[...]).astype(bf16)
@@ -749,6 +772,28 @@
 
     def share(place, part):
         return rows_to(place, part, ad_ss.at[place * parts + part], ad_rs, sp, 1 - tp)
+
+    def up_ready():
+        local_up.wait()
+        for step in range(levels):
+            for way in range(2):
+                diagonal(0, step, step * 4 + 3 - spot, way, 0).wait_recv()
+
+    def lift(block):
+        count = levels // 2
+        for place in range(count):
+            for part in range(parts):
+                share(block * count + place, part).wait_recv()
+        up_whole = (shards * up.shape[1], unit)
+        at = pl.ds(pl.multiple_of(block * count * rows_own, count * rows_own), count * rows_own)
+
+        def one(core, carry):
+            rows = acts[core, pl.ds(block * count, count)].reshape(count * rows_own, model)
+            lifted = jnp.maximum(contract(rows, up[...].reshape(up_whole), ((1,), (0,))), 0.0)
+            hidden[core, at, :] = (lifted * lifted).astype(bf16)
+            return carry
+
+        lax.fori_loop(0, 2, one, 0)
 
     def send_along(hop, part):
         @pl.when((level >= hop) & (level < top))
@@ -781,31 +826,12 @@
                     share(place, part).start()
 
         issue(3 + 10 * hop)
+        if hop == levels - 2:
+            up_ready()
+            lift(level // 2)
     issue(5)
-    phase("side_wait")
-    for place in range(levels):
-        for part in range(parts):
-            share(place, part).wait_recv()
-    issue(6)
-
-    phase("up_wait")
-    local_up.wait()
-    for step in range(levels):
-        for way in range(2):
-            diagonal(0, step, step * 4 + 3 - spot, way, 0).wait_recv()
     phase("lift")
-    up_whole = (shards * up.shape[1], unit)
-
-    def lift(index, carry):
-        core, block = index // 2, lax.rem(index, 2)
-        count = levels // 2
-        rows = acts[core, pl.ds(block * count, count)].reshape(count * rows_own, model)
-        lifted = jnp.maximum(contract(rows, up[...].reshape(up_whole), ((1,), (0,))), 0.0)
-        at = pl.ds(pl.multiple_of(block * count * rows_own, count * rows_own), count * rows_own)
-        hidden[core, at, :] = (lifted * lifted).astype(bf16)
-        return carry
-
-    lax.fori_loop(0, 4, lift, 0)
+    lift(1 - level // 2)
     issue(7)
 
     phase("lower")
@@ -860,11 +886,10 @@
         for k in range(1, levels):
             depth_copy(t, k).wait_recv()
             summed = summed + depth_in[t, k].astype(f32)
-        summed = summed.astype(bf16).astype(f32)
+        summed = summed.astype(bf16)
         for place, source in enumerate(pair_sources(t)):
             at = pl.ds(pl.multiple_of(source * lanes, lanes), lanes)
-            total = state_rows[:, at].astype(f32) + summed[:, place * lanes : (place + 1) * lanes]
-            out_ref[:, at] = total.astype(bf16)
+            out_ref[:, at] = summed[:, place * lanes : (place + 1) * lanes]
 
     count = shards // 2
 
@@ -946,7 +971,7 @@
     ur, dr = ([("rise", kind, step) for step in range(1, levels)] for kind in range(2))
     us, ds = ([("spread", kind, step) for step in range(levels)] for kind in range(2))
     ut, dt = ([("relay", kind, step) for step in range(levels)] for kind in range(2))
-    return {0: [('rise', 0, 1), ('rise', 0, 2), ('spread', 0, 0)], 1: [('rise', 0, 3), ('relay', 0, 0), ('spread', 1, 0), ('spread', 0, 1)], 3: [('relay', 1, 0), ('rise', 1, 1), ('rise', 1, 2), ('rise', 1, 3), ('spread', 0, 2), ('spread', 0, 3)], 4: [('relay', 0, 1), ('relay', 0, 2), ('relay', 0, 3)], 13: [('spread', 1, 1), ('spread', 1, 2), ('spread', 1, 3)], 50: [('relay', 1, 1)], 51: [('relay', 1, 2)], 52: [('relay', 1, 3)]}
+    return {0: [('rise', 0, 1), ('rise', 0, 2), ('spread', 0, 0)], 1: [('rise', 0, 3), ('relay', 0, 0), ('spread', 1, 0), ('spread', 0, 1)], 3: [('relay', 1, 0), ('rise', 1, 1), ('rise', 1, 2), ('rise', 1, 3), ('spread', 0, 2), ('spread', 0, 3)], 4: [('relay', 0, 1), ('relay', 0, 2), ('relay', 0, 3)], 13: [('spread level', 1, 0), ('spread level', 1, 1), ('spread level', 1, 2), ('spread level', 1, 3)], 50: [('relay level', 1, 0)], 51: [('relay level', 1, 1)], 52: [('relay level', 1, 2)], 53: [('relay level', 1, 3)]}
 
 
 def per_device_fused(team, *operands):
@@ -1012,7 +1037,6 @@
         pltpu.VMEM((length, inner), bf16),
         pltpu.VMEM((2, rows_own, model), bf16),
         pltpu.VMEM((rows_own, model), bf16),
-        pltpu.VMEM((rows_own, model), bf16),
         pltpu.VMEM((2, levels, rows_own, model), bf16),
         pltpu.VMEM((2, levels * rows_own, unit), bf16),
         pltpu.VMEM((pairs, levels * rows_own, 2 * lanes), bf16),
@@ -1045,11 +1069,11 @@
         dma((pairs, levels)),
         dma((pairs, levels)),
     ]
-    return pl.pallas_call(
+    state, mixed = pl.pallas_call(
         functools.partial(layer_kernel, team),
-        out_shape=jax.ShapeDtypeStruct((rows_own, model), bf16),
+        out_shape=[jax.ShapeDtypeStruct((rows_own, model), bf16)] * 2,
         in_specs=specs,
-        out_specs=vmem,
+        out_specs=[vmem, vmem],
         scratch_shapes=scratch,
         compiler_params=pltpu.CompilerParams(
             collective_id=0, has_side_effects=True, vmem_limit_bytes=63 * 1024 * 1024
@@ -1073,6 +1097,7 @@
         widening_matrix,
         narrowing_matrix,
     )
+    return (state.astype(f32) + mixed.astype(f32)).astype(bf16)
 
 
 def general_solution(mesh):

time: 111 us -> 110 us (level)
  other arithmetic: 0 us -> 1.8 us
  local copies, waits for them, and re-layouts: 1.67 us -> 0 us
    convert_element_type x0 -> x1, other arithmetic: none -> 1.8 us  [per_device_fused(): return (state.astype(f32) + mixed.astype(f32)).astype(bf16)]
    unnamed x1 -> x0, local copies, waits for them, and re-layouts: 1.67 us -> none
where the time goes in v4:
time: 110 us; the launch traced here: 109 us
  Pallas kernels  108 us (98%)
  other arithmetic  1.8 us (2%)
    pallas_call x1, Pallas kernels, per_device_fused(): pl.pallas_call(functools.partial(layer_kernel, team), out_shape=[jax.Shap...  108 us

profile of v4, /device:TPU:0, one launch (start us, length us, event | category | flops | bytes accessed | tf_op | source)
XLA Modules:
  0.0 109.5 jit_solution(5676268606126297089)
XLA Ops:
  0.0 107.7 %shard_map.163 = (bf16[64,2048]{1,0:T(8,128)(2,1)}, bf16[64,2048]{1,0:T(8,128)(2,1)}) custom-call(bf16[64,2048]{1,0:T(8,128)(2,1)} %skip_hbm.1, bf16[128,2048]{1,0:T(8,128)(2,1)} %content_hbm.1, bf16[128,512]{1,0:T(8,128)(2,1)} %writer_hbm.1, bf16[128,512]{1,0:T(8,128)(2,1)} %reader_hbm.1, bf16[128,2048]{1,0:T(8,128)(2,1)} %multiplier_hbm.1, ...), custom_call_target="tpu_custom_call" | custom-call | tf_op jit(solution)/shard_map/pallas_call | solution.py:1072
  107.7 1.8 %add_convert_fusion = bf16[64,2048]{1,0:T(8,128)(2,1)} fusion(bf16[64,2048]{1,0:T(8,128)(2,1)} %get-tuple-element.8, bf16[64,2048]{1,0:T(8,128)(2,1)} %get-tuple-element.7), kind=kLoop, calls=%fused_computation | loop fusion | flops 524288 | bytes 786432 | tf_op jit(solution)/shard_map/convert_element_type | solution.py:1100

commit v5 on v4

--- a/solution.py
+++ b/solution.py
@@ -894,6 +894,11 @@
     count = shards // 2
 
     def stage(t, carry):
+        @pl.when((t >= 1) & (t < count + 1))
+        def _():
+            with jax.named_scope("pair_step"):
+                pair_step(t - 1)
+
         for turn in range(levels + 1):
             if batches.get(50 + turn):
 
@@ -905,11 +910,6 @@
         def _():
             with jax.named_scope("lower_step"):
                 lower_step(t)
-
-        @pl.when((t >= 1) & (t < count + 1))
-        def _():
-            with jax.named_scope("pair_step"):
-                pair_step(t - 1)
 
         @pl.when(t >= LAG)
         def _():

time: 110 us -> 108 us (0.982)
  Pallas kernels: 108 us -> 106 us
    pallas_call x1, Pallas kernels: 108 us -> 106 us  [per_device_fused(): pl.pallas_call(functools.partial(layer_kernel, team), out_shape=[jax.Shap...]
where the time goes in v5:
time: 108 us
  Pallas kernels  106 us (98%)
  other arithmetic  1.8 us (2%)
    pallas_call x1, Pallas kernels, per_device_fused(): pl.pallas_call(functools.partial(layer_kernel, team), out_shape=[jax.Shap...  106 us

profile of v5, /device:TPU:0, one launch (start us, length us, event | category | flops | bytes accessed | tf_op | source)
XLA Modules:
  0.0 107.6 jit_solution(6098863639408975416)
XLA Ops:
  0.0 105.8 %shard_map.163 = (bf16[64,2048]{1,0:T(8,128)(2,1)}, bf16[64,2048]{1,0:T(8,128)(2,1)}) custom-call(bf16[64,2048]{1,0:T(8,128)(2,1)} %skip_hbm.1, bf16[128,2048]{1,0:T(8,128)(2,1)} %content_hbm.1, bf16[128,512]{1,0:T(8,128)(2,1)} %writer_hbm.1, bf16[128,512]{1,0:T(8,128)(2,1)} %reader_hbm.1, bf16[128,2048]{1,0:T(8,128)(2,1)} %multiplier_hbm.1, ...), custom_call_target="tpu_custom_call" | custom-call | tf_op jit(solution)/shard_map/pallas_call | solution.py:1072
  105.8 1.8 %add_convert_fusion = bf16[64,2048]{1,0:T(8,128)(2,1)} fusion(bf16[64,2048]{1,0:T(8,128)(2,1)} %get-tuple-element.8, bf16[64,2048]{1,0:T(8,128)(2,1)} %get-tuple-element.7), kind=kLoop, calls=%fused_computation | loop fusion | flops 524288 | bytes 786432 | tf_op jit(solution)/shard_map/convert_element_type | solution.py:1100
